TPU v7x, 32 devices: a whole 2x2x4 slice. The times are simulated.
32 devices in a mesh: sp: 8 (over z, y), tp: 4 (over x, core).
Axes of the slice: x: 2, y: 2, z: 4, core: 2. Of those that a mesh axis runs over, the one named last changes fastest.
Arguments:
- cotangent: bfloat16 [2048, 2048], P('sp'), may hold values from -6 to 6
- stream_in: bfloat16 [2048, 2048], P('sp'), may hold values from -6 to 6
- norm_gain: float32 [2048], replicated, may hold values from 0.1 to 1.9
- out_gate: bfloat16 [2048, 1024], P('sp', 'tp'), may hold values from -6 to 6
- in_gate: bfloat16 [2048, 1024], P('sp', 'tp'), may hold values from -6 to 6
- conv_input: bfloat16 [2048, 1024], P('sp', 'tp'), may hold values from -6 to 6
- conv_taps: float32 [3, 1024], P(None, 'tp'), may hold values from -3 to 3
- out_weight: bfloat16 [2048, 1024], P(None, 'tp'), may hold values from -0.1875 to 0.1875
- expert_gate: bfloat16 [8, 2048, 1024], P('sp', None, 'tp'), may hold values from -0.125 to 0.125
- expert_up: bfloat16 [8, 2048, 1024], P('sp', None, 'tp'), may hold values from -0.125 to 0.125
- expert_down: bfloat16 [8, 1024, 2048], P('sp', 'tp'), may hold values from -0.1875 to 0.1875
- expert_choice: int32 [2048, 2], P('sp'), may hold values from 0 to 7, all different within a row; in each aligned block of 256 rows (0 to 255, 256 to 511, ...) at most 128 rows name the same one
- route_scale: float32 [2048, 2], P('sp'), may hold values from 0.05 to 0.6
Outputs:
- grad_stream: bfloat16 [2048, 2048], P('sp', 'tp')
- grad_out_gate: bfloat16 [2048, 1024], P('sp', 'tp')
- grad_in_gate: bfloat16 [2048, 1024], P('sp', 'tp')
- grad_conv_input: bfloat16 [2048, 1024], P('sp', 'tp')
- grad_out_weight: float32 [2048, 1024], P('sp', 'tp')
- grad_expert_gate: float32 [8, 2048, 1024], P('sp', None, 'tp')
- grad_expert_up: float32 [8, 2048, 1024], P('sp', None, 'tp')
- grad_expert_down: float32 [8, 1024, 2048], P('sp', 'tp')
Inputs may be any that keep to these rules, and one draw needn't show every extreme that they name: `expert_choice`: each row names two different experts. Within the rows of one device no expert is named more than 128 times, a bound that some block reaches in some devices' rows.
All inputs are finite; a program needn't handle non-finite values.
Results may differ from a plain program's by a relative error of at most 0.01.
Values may be sent and summed in bfloat16 or wider, within the bound.
A program may use at most 128 MiB of HBM per device.

v0:
```python
import functools

import jax
import jax.numpy as jnp
from jax import lax
from jax.experimental import pallas as pl
from jax.experimental.pallas import tpu as pltpu
from jax.sharding import PartitionSpec as P

norm_eps = 1e-06


def passed_along(value, axis, steps):
    count = lax.axis_size(axis)
    first, last = (max(0, -steps), min(count, count - steps))
    return lax.ppermute(value, axis, [(source, source + steps) for source in range(first, last)])


def slot_masks(choice_rows, expert_count, capacity):
    rows = choice_rows.shape[0]
    onehot = choice_rows[:, :, None] == jnp.arange(expert_count, dtype=jnp.int32)
    member = jnp.any(onehot, axis=1).astype(jnp.bfloat16)
    at = jnp.arange(rows, dtype=jnp.int32)
    before = (at[:, None] > at[None, :]).astype(jnp.bfloat16)
    earlier = jnp.dot(before, member, preferred_element_type=jnp.float32).astype(jnp.int32)
    position = jnp.sum(jnp.where(onehot, earlier[:, None, :], 0), axis=-1)
    slot = choice_rows * capacity + position
    slots = jnp.arange(expert_count * capacity, dtype=jnp.int32)[:, None]
    return (slots == slot[:, 0][None, :], slots == slot[:, 1][None, :])


def rows_product(left, right):
    return lax.dot_general(
        left, right, (((0,), (0,)), ((), ())), preferred_element_type=jnp.float32
    )


def cols_product(left, right):
    return lax.dot_general(
        left, right, (((1,), (1,)), ((), ())), preferred_element_type=jnp.float32
    )


MESH = pl.DeviceIdType.MESH


def remote(source, target, send_sem, recv_sem, device):
    return pltpu.make_async_remote_copy(
        src_ref=source,
        dst_ref=target,
        send_sem=send_sem,
        recv_sem=recv_sem,
        device_id=device,
        device_id_type=MESH,
    )


def columns(index, width):
    return pl.ds(pl.multiple_of(index * width, width), width)


def mirrored(me, mask, n):
    found, unit = 0, 1
    while unit < n:
        found = found + lax.rem(lax.div(me, unit) + lax.div(mask, unit), 2) * unit
        unit = 2 * unit
    return found


def tp_places():
    tp, count = lax.axis_index("tp"), lax.axis_size("tp")
    cross = lax.rem(tp + count // 2, count)
    partner = tp + 1 - 2 * lax.rem(tp, 2)
    return (tp, cross, partner, lax.rem(partner + count // 2, count))


def greet(exchange, cross, partner):
    barrier = pltpu.get_barrier_semaphore()
    waits = 2
    for peer in (cross, partner):
        pl.semaphore_signal(barrier, inc=1, device_id={"tp": peer}, device_id_type=MESH)
    if exchange:
        me, n = lax.axis_index("sp"), lax.axis_size("sp")
        waits = waits + n - 1

        def greet_one(k, carry):
            peer = lax.rem(me + k, n)
            pl.semaphore_signal(barrier, inc=1, device_id={"sp": peer}, device_id_type=MESH)
            return carry

        lax.fori_loop(1, n, greet_one, 0)
    pl.semaphore_wait(barrier, waits)


def gather_kernel(n, exchange, count, *refs):
    ins, outs = refs[:count], refs[count : 2 * count]
    local, send, recv_a, recv_b, recv_near = refs[2 * count :]
    rows, width = ins[0].shape
    depth = rows // n
    tp, cross, partner, _ = tp_places()
    me = lax.axis_index("sp")
    greet(exchange, cross, partner)

    def block_of(a, block, column):
        return outs[a].at[pl.ds(pl.multiple_of(block * depth, depth), depth), columns(column, width)]

    def source(k):
        if not exchange:
            return k
        odd = k % 2
        mask = odd * ((k + 1) // 2) + (1 - odd) * ((n - k // 2) % n)
        return mirrored(me, jnp.int32(mask), n)

    def sent(a, k):
        peer = source(k)
        return remote(
            ins[a].at[pl.ds(pl.multiple_of(peer * depth, depth), depth), :],
            block_of(a, me, tp),
            send.at[0, a],
            recv_a.at[a, k],
            {"sp": peer},
        )

    def send_all(k, carry):
        for a in range(count):
            sent(a, k).start()
        return carry

    def across(a, k):
        block = block_of(a, source(k), tp)
        return remote(block, block, send.at[1, a], recv_b.at[a, k], {"tp": cross})

    def relay(k):
        for a in range(count):
            if exchange and not isinstance(k, int):
                sent(a, k).wait_recv()
            block = block_of(a, source(k), tp)
            across(a, k).start()
            remote(block, block, send.at[2, a], recv_near.at[0, a], {"tp": partner}).start()

    def forward(k):
        for a in range(count):
            across(a, k).wait_recv()
            block = block_of(a, source(k), cross)
            remote(block, block, send.at[3, a], recv_near.at[1, a], {"tp": partner}).start()

    if exchange:
        lax.fori_loop(1, n, send_all, 0)
    for a in range(count):
        if exchange:
            own = pltpu.make_async_copy(
                ins[a].at[pl.ds(pl.multiple_of(me * depth, depth), depth), :],
                block_of(a, me, tp),
                local.at[a],
            )
        else:
            own = pltpu.make_async_copy(ins[a], outs[a].at[:, columns(tp, width)], local.at[a])
        own.start()
        own.wait()
    relay(0)

    def step(k, carry):
        relay(k)
        forward(k - 1)
        return carry

    lax.fori_loop(1, n, step, 0)
    forward(n - 1)
    for a in range(count):
        whole = outs[a].at[:, columns(tp, width)]
        for kind in (0, 1):
            remote(whole, whole, send.at[2, a], recv_near.at[kind, a], {"tp": partner}).wait_recv()
        for kind in (1, 2, 3):
            remote(whole, whole, send.at[kind, a], recv_near.at[0, a], {"tp": partner}).wait_send()
        if exchange:
            rest = ins[a].at[pl.ds(0, (n - 1) * depth), :]
            remote(rest, rest, send.at[0, a], recv_near.at[0, a], {"tp": partner}).wait_send()


def gathered(parts, n, exchange, collective_id):
    count = len(parts)
    rows, width = parts[0].shape
    wide = jax.ShapeDtypeStruct((rows, width * lax.axis_size("tp")), parts[0].dtype)
    return pl.pallas_call(
        functools.partial(gather_kernel, n, exchange, count),
        out_shape=[wide] * count,
        in_specs=[pl.BlockSpec(memory_space=pl.ANY)] * count,
        out_specs=[pl.BlockSpec(memory_space=pl.ANY)] * count,
        scratch_shapes=[
            pltpu.SemaphoreType.DMA((count,)),
            pltpu.SemaphoreType.DMA((4, count)),
            pltpu.SemaphoreType.DMA((count, n)),
            pltpu.SemaphoreType.DMA((count, n)),
            pltpu.SemaphoreType.DMA((2, count)),
        ],
        compiler_params=pltpu.CompilerParams(collective_id=collective_id, has_side_effects=True),
    )(*parts)


def return_kernel(
    n,
    partial,
    out,
    near,
    far_out,
    far_in,
    total,
    local,
    send_near,
    recv_near,
    send_far,
    recv_far,
    send_out,
    recv_out,
):
    width = out.shape[2]
    tp, cross, partner, diagonal = tp_places()
    me = lax.axis_index("sp")
    greet(True, cross, partner)

    def target(k):
        return mirrored(me, jnp.int32(n - 1 - k), n)

    def part(k, column):
        return partial[target(k), :, columns(column, width)].astype(jnp.float32)

    def handed(j, k):
        return remote(
            partial.at[target(k), :, columns((partner, diagonal)[j], width)],
            near.at[j, k],
            send_near.at[j],
            recv_near.at[j, k],
            {"tp": partner},
        )

    def across(k):
        return remote(far_out.at[k], far_in.at[k], send_far, recv_far.at[k], {"tp": cross})

    def hand(k, carry):
        handed(1, k).start()
        handed(0, k).start()
        return carry

    def pair(k, carry):
        handed(1, k).wait_recv()
        far_out[k] = (part(k, cross) + near[1, k].astype(jnp.float32)).astype(far_out.dtype)
        across(k).start()
        return carry

    def finish(k):
        handed(0, k).wait_recv()
        across(k).wait_recv()
        total[k] = (
            part(k, tp) + near[0, k].astype(jnp.float32) + far_in[k].astype(jnp.float32)
        ).astype(total.dtype)

    def finish_remote(k, carry):
        finish(k)
        remote(total.at[k], out.at[me], send_out, recv_out, {"sp": target(k)}).start()
        return carry

    lax.fori_loop(0, n, hand, 0)
    lax.fori_loop(0, n, pair, 0)
    lax.fori_loop(0, n - 1, finish_remote, 0)
    finish(n - 1)
    own = pltpu.make_async_copy(total.at[n - 1], out.at[me], local)
    own.start()
    own.wait()
    rest, rest_out = total.at[pl.ds(0, n - 1)], out.at[pl.ds(0, n - 1)]
    remote(rest, rest_out, send_out, recv_out, {"tp": partner}).wait()
    remote(far_out, far_in, send_far, recv_out, {"tp": cross}).wait_send()
    for j in (0, 1):
        remote(far_out, near.at[j], send_near.at[j], recv_out, {"tp": partner}).wait_send()


def returned_slots(partial, n, collective_id):
    rows, wide = partial.shape
    width, depth = wide // lax.axis_size("tp"), rows // n
    kind = partial.dtype
    return pl.pallas_call(
        functools.partial(return_kernel, n),
        out_shape=jax.ShapeDtypeStruct((n, depth, width), kind),
        in_specs=[pl.BlockSpec(memory_space=pltpu.VMEM)],
        out_specs=pl.BlockSpec(memory_space=pl.ANY),
        scratch_shapes=[
            pltpu.VMEM((2, n, depth, width), kind),
            pltpu.VMEM((n, depth, width), kind),
            pltpu.VMEM((n, depth, width), kind),
            pltpu.VMEM((n, depth, width), kind),
            pltpu.SemaphoreType.DMA,
            pltpu.SemaphoreType.DMA((2,)),
            pltpu.SemaphoreType.DMA((2, n)),
            pltpu.SemaphoreType.DMA,
            pltpu.SemaphoreType.DMA((n,)),
            pltpu.SemaphoreType.DMA,
            pltpu.SemaphoreType.DMA,
        ],
        compiler_params=pltpu.CompilerParams(
            collective_id=collective_id, has_side_effects=True, vmem_limit_bytes=32 * 1024 * 1024
        ),
    )(partial.reshape(n, depth, wide)).reshape(rows, width)


def shards(
    cotangent,
    stream_in,
    norm_gain,
    out_gate,
    in_gate,
    conv_input,
    conv_taps,
    out_weight,
    expert_gate,
    expert_up,
    expert_down,
    expert_choice,
    route_scale,
):
    sp_size = lax.axis_size("sp")
    tp_size = lax.axis_size("tp")
    rows_here = stream_in.shape[0]
    model_width = stream_in.shape[1]
    column_width = model_width // tp_size
    column_start = lax.axis_index("tp") * column_width
    capacity = 4 * rows_here // sp_size
    stream = stream_in.astype(jnp.float32)
    inverse_rms = lax.rsqrt(jnp.mean(stream * stream, axis=-1, keepdims=True) + norm_eps)
    unit_stream = stream * inverse_rms
    normed = (unit_stream * norm_gain).astype(jnp.bfloat16)
    first, second = slot_masks(expert_choice, sp_size, capacity)
    placing = (first | second).astype(jnp.bfloat16)
    weight = jnp.sum(
        jnp.where(first, route_scale[:, 0][None, :], 0.0)
        + jnp.where(second, route_scale[:, 1][None, :], 0.0),
        axis=1,
    )
    cot_cols = lax.dynamic_slice_in_dim(cotangent, column_start, column_width, 1)
    normed_cols = lax.dynamic_slice_in_dim(normed, column_start, column_width, 1)
    scaled_part = (
        jnp.dot(placing, cot_cols, preferred_element_type=jnp.float32) * weight[:, None]
    ).astype(jnp.bfloat16)
    rows_part = jnp.dot(placing, normed_cols, preferred_element_type=jnp.float32).astype(
        jnp.bfloat16
    )
    expert_rows, scaled_cot = gathered((rows_part, scaled_part), sp_size, True, 1)
    w_gate = expert_gate[0]
    w_up = expert_up[0]
    w_down = expert_down[0]
    gate_pre = jnp.dot(expert_rows, w_gate, preferred_element_type=jnp.float32)
    up_pre = jnp.dot(expert_rows, w_up, preferred_element_type=jnp.float32)
    sigmoid_gate = jax.nn.sigmoid(gate_pre)
    silu_gate = gate_pre * sigmoid_gate
    hidden = (silu_gate * up_pre).astype(jnp.bfloat16)
    hidden_grad = cols_product(scaled_cot, w_down)
    gate_grad = (
        hidden_grad * up_pre * sigmoid_gate * (1.0 + gate_pre * (1.0 - sigmoid_gate))
    ).astype(jnp.bfloat16)
    up_grad = (hidden_grad * silu_gate).astype(jnp.bfloat16)
    partial_grad = cols_product(gate_grad, w_gate) + cols_product(up_grad, w_up)
    returned = returned_slots(partial_grad.astype(jnp.bfloat16), sp_size, 2)
    grad_down = rows_product(hidden, scaled_cot)[None]
    grad_gate = rows_product(expert_rows, gate_grad)[None]
    grad_up = rows_product(expert_rows, up_grad)[None]
    product = in_gate.astype(jnp.float32) * conv_input.astype(jnp.float32)
    earlier = passed_along(product[-2:], "sp", 1)
    extended = jnp.concatenate([earlier, product], axis=0)
    filtered = conv_taps[0] * product + conv_taps[1] * extended[1:-1] + conv_taps[2] * extended[:-2]
    mixed_in = (out_gate.astype(jnp.float32) * filtered).astype(jnp.bfloat16)
    token_cols = rows_product(placing, returned).astype(jnp.bfloat16)
    pieces = max(1, rows_here // 64)
    (token_grad,) = gathered((token_cols,), pieces, False, 3)
    unit_grad = token_grad.astype(jnp.float32) * norm_gain
    along = jnp.mean(unit_stream * unit_grad, axis=-1, keepdims=True)
    stream_grad = (
        cotangent.astype(jnp.float32) + inverse_rms * (unit_grad - unit_stream * along)
    ).astype(jnp.bfloat16)
    grad_stream = lax.dynamic_slice_in_dim(stream_grad, column_start, column_width, 1)
    mixed_grad = jnp.dot(stream_grad, out_weight, preferred_element_type=jnp.float32)
    grad_out_gate = (mixed_grad * filtered).astype(jnp.bfloat16)
    filtered_grad = mixed_grad * out_gate.astype(jnp.float32)
    later = passed_along(filtered_grad[:2], "sp", -1)
    extended_grad = jnp.concatenate([filtered_grad, later], axis=0)
    product_grad = (
        conv_taps[0] * filtered_grad
        + conv_taps[1] * extended_grad[1:-1]
        + conv_taps[2] * extended_grad[2:]
    )
    grad_in_gate = (product_grad * conv_input.astype(jnp.float32)).astype(jnp.bfloat16)
    grad_conv_input = (product_grad * in_gate.astype(jnp.float32)).astype(jnp.bfloat16)
    shares = rows_product(stream_grad, mixed_in).astype(jnp.bfloat16)
    shares = shares.reshape(sp_size, model_width // sp_size, -1)
    shares = lax.all_to_all(shares, "sp", split_axis=0, concat_axis=0)
    grad_out_weight = jnp.sum(shares.astype(jnp.float32), axis=0)
    return (
        grad_stream,
        grad_out_gate,
        grad_in_gate,
        grad_conv_input,
        grad_out_weight,
        grad_gate,
        grad_up,
        grad_down,
    )


def solution(mesh):
    placed = (
        P("sp", None),
        P("sp", None),
        P(),
        P("sp", "tp"),
        P("sp", "tp"),
        P("sp", "tp"),
        P(None, "tp"),
        P(None, "tp"),
        P("sp", None, "tp"),
        P("sp", None, "tp"),
        P("sp", "tp", None),
        P("sp", None),
        P("sp", None),
    )
    return jax.shard_map(
        shards,
        mesh=mesh,
        in_specs=placed,
        out_specs=(
            P("sp", "tp"),
            P("sp", "tp"),
            P("sp", "tp"),
            P("sp", "tp"),
            P("sp", "tp"),
            P("sp", None, "tp"),
            P("sp", None, "tp"),
            P("sp", "tp", None),
        ),
        check_vma=False,
    )
```

profile of v0, /device:TPU:0, one launch (start us, length us, event | category | flops | bytes accessed | tf_op | source)
XLA Modules:
  0.0 182.6 jit_solution(4258085288601916786)
XLA Ops:
  0.6 0.0 copy-start
  0.6 0.0 copy-start.1
  0.7 1.1 convert_multiply_fusion.6
  1.8 4.9 %collective-permute-start = (f32[2,256]{1,0:T(2,128)S(1)}, f32[2,256]{1,0:T(2,128)S(1)}, u32[]{:S(2)}, u32[]{:S(2)}) collective-permute-start(f32[2,256]{1,0:T(2,128)S(1)} %slice.57), channel_id=1, source_target_pairs={{0,4},{4,8},{8,12},{12,16},{16,20},{20,24},{24,28},{1,5},{5,9},{9,... | collective-permute-start | bytes 6152 | tf_op jit(solution)/shard_map/ppermute | solution.py:16
  6.7 0.0 copy-start.12
  6.7 1.5 fusion
  8.3 0.7 fusion.40
  9.0 0.8 fusion.47
  9.7 0.2 convolution_convert_fusion.3
  9.9 0.7 select_reduce_fusion
  10.6 0.7 multiply_add_fusion
  11.3 0.0 copy-done.1
  11.3 1.5 convert_multiply_fusion
  12.8 0.0 copy-done.12
  12.8 0.1 dynamic-slice
  12.9 0.3 add_reduce_fusion
  13.2 2.4 %multiply_convert_fusion.refs_1_ = bf16[1024,512]{1,0:T(8,128)(2,1)} fusion(f32[1024]{0:T(1024)S(1)} %add_reduce_fusion, s32[256]{0:T(256)S(1)} %bitcast.60, s32[256]{0:T(256)S(1)} %bitcast.56, bf16[256,2048]{1,0:T(8,128)(2,1)} %param.13, s32[]{:T(128)S(6)} %select_n.17), kind=kOutput, calls=%fused_computation.12 | convolution fusion | flops 270270464 | bytes 1316868 | tf_op jit(solution)/shard_map/dot_general | solution.py:340
  15.6 2.5 %convolution_convert_fusion.1.refs_0_ = bf16[1024,512]{1,0:T(8,128)(2,1)} fusion(s32[256]{0:T(256)S(1)} %bitcast.61, s32[256]{0:T(256)S(1)} %bitcast.57, f32[256,2048]{1,0:T(8,128)} %convert_multiply_fusion, s32[]{:T(128)S(6)} %select_n.17, f32[512]{0:T(512)S(1)} %dynamic-slice), kind=kOutput, calls=%fused_computation.13 | convolution fusion | flops 270008320 | bytes 1576964 | tf_op jit(solution)/shard_map/dot_general | solution.py:342
  18.0 62.4 %shard_map.188 = (bf16[1024,2048]{1,0:T(8,128)(2,1)}, bf16[1024,2048]{1,0:T(8,128)(2,1)}) custom-call(bf16[1024,512]{1,0:T(8,128)(2,1)} %convolution_convert_fusion.1.refs_0_, bf16[1024,512]{1,0:T(8,128)(2,1)} %multiply_convert_fusion.refs_1_), custom_call_target="tpu_custom_call" | custom-call | tf_op jit(solution)/shard_map/pallas_call | solution.py:184
  80.4 0.0 copy-done
  80.4 0.0 copy-start.3
  80.4 3.6 %fusion.3 = f32[1024,256]{1,0:T(8,128)S(1)} fusion(bf16[1024,2048]{1,0:T(8,128)(2,1)} %get-tuple-element.11, bf16[1,2048,256]{2,1,0:T(8,128)(2,1)S(1)} %copy-done), kind=kOutput, calls=%fused_computation.18 | convolution fusion | flops 1073741824 | bytes 6291456 | tf_op jit(solution)/shard_map/dot_general | solution.py:349
  84.1 0.1 copy-done.16
  84.2 1.3 fusion.6
  85.5 0.0 copy-start.22
  85.5 1.7 copy-done.14
  87.1 0.3 copy-done.18
  87.4 1.6 multiply_convert_fusion.2
  89.0 0.0 copy-start.5
  89.1 1.3 fusion.1
  90.4 1.3 add_convert_fusion
  91.7 32.9 %shard_map.189 = bf16[8,128,512]{2,1,0:T(8,128)(2,1)S(1)} custom-call(bf16[8,128,2048]{2,1,0:T(8,128)(2,1)S(1)} %bitcast.46), custom_call_target="tpu_custom_call" | custom-call | tf_op jit(solution)/shard_map/pallas_call | solution.py:280
  124.6 1.2 convolution_convert_fusion.2.refs_0_
  125.8 19.8 %shard_map.190 = bf16[256,2048]{1,0:T(8,128)(2,1)} custom-call(bf16[256,512]{1,0:T(8,128)(2,1)} %convolution_convert_fusion.2.refs_0_), custom_call_target="tpu_custom_call" | custom-call | tf_op jit(solution)/shard_map/pallas_call | solution.py:184
  145.6 0.0 copy-start.2
  145.6 0.0 copy-start.4
  145.6 1.9 %multiply_reduce_fusion = f32[256]{0:T(256)S(1)} fusion(bf16[256,2048]{1,0:T(8,128)(2,1)} %shard_map.190, f32[2048]{0:T(1024)S(1)} %copy-done.12, f32[256]{0:T(256)S(1)} %add_rsqrt_fusion, bf16[256,2048]{1,0:T(8,128)(2,1)S(1)} %copy-done.1), kind=kLoop, calls=%fused_computation.10 | loop fusion | flops 3145472 | bytes 2107392 | tf_op jit(solution)/shard_map/reduce_sum | solution.py:373
  147.5 0.0 copy-done.2
  147.5 0.0 copy-done.4
  147.5 0.0 copy-start.13
  147.6 0.0 copy-start.11
  147.6 0.0 copy-start.19
  147.6 0.8 add_convert_fusion.1
  148.4 0.0 collective-permute-done
  148.4 0.0 copy-done.11
  148.5 0.4 copy-done.19
  148.9 1.2 multiply_convert_fusion.5
  150.1 1.5 convolution_convert_fusion
  151.5 3.9 %all-to-all-start = ((bf16[8,256,256]{2,1,0:T(8,128)(2,1)}), bf16[8,256,256]{2,1,0:T(8,128)(2,1)S(1)}, u32[]{:S(2)}, u32[]{:S(2)}) async-start(bf16[8,256,256]{2,1,0:T(8,128)(2,1)} %bitcast.48), calls=%async_computation | async-start | bytes 2097152 | tf_op jit(solution)/shard_map/all_to_all | solution.py:392
  155.5 0.0 copy-start.17
  155.5 5.1 %convolution_bitcast_fusion.1 = f32[1,2048,256]{2,1,0:T(8,128)} fusion(bf16[1024,2048]{1,0:T(8,128)(2,1)} %get-tuple-element.11, bf16[1024,256]{1,0:T(8,128)(2,1)} %copy-done.7), kind=kOutput, calls=%fused_computation.2 | convolution fusion | flops 1073741824 | bytes 6815744 | tf_op jit(solution)/shard_map/dot_general | solution.py:33
  160.6 0.0 copy-done.17
  160.6 0.0 copy-start.23
  160.6 2.7 %convolution_bitcast_fusion.2 = f32[1,2048,256]{2,1,0:T(8,128)} fusion(bf16[1024,2048]{1,0:T(8,128)(2,1)S(1)} %copy-done.17, bf16[1024,256]{1,0:T(8,128)(2,1)S(1)} %copy-done.6), kind=kOutput, calls=%fused_computation.3 | convolution fusion | flops 1073741824 | bytes 6815744 | tf_op jit(solution)/shard_map/dot_general | solution.py:33
  163.3 0.1 copy-done.21
  163.5 0.7 copy-done.23
  164.2 2.7 %convolution_bitcast_fusion = f32[1,256,2048]{2,1,0:T(8,128)} fusion(bf16[1024,2048]{1,0:T(8,128)(2,1)S(1)} %copy-done.15, f32[1024,256]{1,0:T(8,128)S(1)} %copy-done.23, f32[1024,256]{1,0:T(8,128)S(1)} %copy-done.21), kind=kOutput, calls=%fused_computation.1 | convolution fusion | flops 1075314688 | bytes 8388608 | tf_op jit(solution)/shard_map/dot_general | solution.py:33
  166.8 1.3 collective-permute-start.1
  168.1 0.7 constant_dynamic-slice_fusion
  168.8 3.5 %collective-permute-done.1 = f32[2,256]{1,0:T(2,128)S(1)} collective-permute-done((f32[2,256]{1,0:T(2,128)S(1)}, f32[2,256]{1,0:T(2,128)S(1)}, u32[]{:S(2)}, u32[]{:S(2)}) %collective-permute-start.1) | collective-permute-done | bytes 2080 | tf_op jit(solution)/shard_map/ppermute | solution.py:16
  172.3 0.8 fusion.30
  173.1 0.7 fusion.31
  173.7 8.0 %all-to-all-done = bf16[8,256,256]{2,1,0:T(8,128)(2,1)S(1)} async-done(((bf16[8,256,256]{2,1,0:T(8,128)(2,1)}), bf16[8,256,256]{2,1,0:T(8,128)(2,1)S(1)}, u32[]{:S(2)}, u32[]{:S(2)}) %all-to-all-start) | async-done | bytes 1048608 | tf_op jit(solution)/shard_map/all_to_all | solution.py:392
  181.8 0.8 convert_reduce_fusion
  (28 shorter events, 0.1 us)
Async XLA Ops:
  0.6 79.8 %copy-start = (bf16[1,2048,256]{2,1,0:T(8,128)(2,1)S(1)}, bf16[1,2048,256]{2,1,0:T(8,128)(2,1)}, u32[]{:S(2)}) copy-start(bf16[1,2048,256]{2,1,0:T(8,128)(2,1)} %param.21) | copy-start | bytes 3145732
  0.6 10.7 %copy-start.1 = (bf16[256,2048]{1,0:T(8,128)(2,1)S(1)}, bf16[256,2048]{1,0:T(8,128)(2,1)}, u32[]{:S(2)}) copy-start(bf16[256,2048]{1,0:T(8,128)(2,1)} %param.14) | copy-start | bytes 3145732
  1.8 146.6 %collective-permute-start = (f32[2,256]{1,0:T(2,128)S(1)}, f32[2,256]{1,0:T(2,128)S(1)}, u32[]{:S(2)}, u32[]{:S(2)}) collective-permute-start(f32[2,256]{1,0:T(2,128)S(1)} %slice.57), channel_id=1, source_target_pairs={{0,4},{4,8},{8,12},{12,16},{16,20},{20,24},{24,28},{1,5},{5,9},{9,... | collective-permute-start | bytes 6152 | tf_op jit(solution)/shard_map/ppermute | solution.py:16
  6.7 6.1 %copy-start.12 = (f32[2048]{0:T(1024)S(1)}, f32[2048]{0:T(1024)}, u32[]{:S(2)}) copy-start(f32[2048]{0:T(1024)} %param.15) | copy-start | bytes 24580
  80.4 3.6 %copy-start.3 = (bf16[1,2048,256]{2,1,0:T(8,128)(2,1)S(1)}, bf16[1,2048,256]{2,1,0:T(8,128)(2,1)}, u32[]{:S(2)}) copy-start(bf16[1,2048,256]{2,1,0:T(8,128)(2,1)} %param.22) | copy-start | bytes 3145732
  80.4 3.8 %copy-start.16 = (bf16[1024,2048]{1,0:T(8,128)(2,1)S(1)}, bf16[1024,2048]{1,0:T(8,128)(2,1)}, u32[]{:S(2)}) copy-start(bf16[1024,2048]{1,0:T(8,128)(2,1)} %get-tuple-element.11) | copy-start | bytes 12582916
  84.2 1.3 copy-start.20
  84.2 2.9 %copy-start.14 = (bf16[1024,2048]{1,0:T(8,128)(2,1)S(1)}, bf16[1024,2048]{1,0:T(8,128)(2,1)}, u32[]{:S(2)}) copy-start(bf16[1024,2048]{1,0:T(8,128)(2,1)} %get-tuple-element.10) | copy-start | bytes 12582916
  84.2 3.2 %copy-start.18 = (bf16[1,256,2048]{2,1,0:T(8,128)(2,1)S(1)}, bf16[1,256,2048]{2,1,0:T(8,128)(2,1)}, u32[]{:S(2)}) copy-start(bf16[1,256,2048]{2,1,0:T(8,128)(2,1)} %param.23) | copy-start | bytes 3145732
  85.5 3.6 %copy-start.22 = (f32[1024,256]{1,0:T(8,128)}, f32[1024,256]{1,0:T(8,128)S(1)}, u32[]{:S(2)}) copy-start(f32[1024,256]{1,0:T(8,128)S(1)} %fusion.6) | copy-start | bytes 3145732
  89.0 1.3 copy-start.5
  89.1 1.3 copy-start.7
  145.6 2.0 %copy-start.2 = (bf16[256,2048]{1,0:T(8,128)(2,1)S(1)}, bf16[256,2048]{1,0:T(8,128)(2,1)}, u32[]{:S(2)}) copy-start(bf16[256,2048]{1,0:T(8,128)(2,1)} %shard_map.190) | copy-start | bytes 3145732
  145.6 2.0 %copy-start.4 = (bf16[256,2048]{1,0:T(8,128)(2,1)S(1)}, bf16[256,2048]{1,0:T(8,128)(2,1)}, u32[]{:S(2)}) copy-start(bf16[256,2048]{1,0:T(8,128)(2,1)} %param.13) | copy-start | bytes 3145732
  147.5 0.8 copy-start.13
  147.6 0.9 copy-start.11
  147.6 1.3 copy-start.19
  151.5 30.3 %all-to-all-start = ((bf16[8,256,256]{2,1,0:T(8,128)(2,1)}), bf16[8,256,256]{2,1,0:T(8,128)(2,1)S(1)}, u32[]{:S(2)}, u32[]{:S(2)}) async-start(bf16[8,256,256]{2,1,0:T(8,128)(2,1)} %bitcast.48), calls=%async_computation | async-start | bytes 2097152 | tf_op jit(solution)/shard_map/all_to_all | solution.py:392
  155.5 5.1 %copy-start.6 = (bf16[1024,256]{1,0:T(8,128)(2,1)S(1)}, bf16[1024,256]{1,0:T(8,128)(2,1)}, u32[]{:S(2)}) copy-start(bf16[1024,256]{1,0:T(8,128)(2,1)} %copy-done.5) | copy-start | bytes 1572868
  155.5 5.1 %copy-start.17 = (bf16[1024,2048]{1,0:T(8,128)(2,1)S(1)}, bf16[1024,2048]{1,0:T(8,128)(2,1)}, u32[]{:S(2)}) copy-start(bf16[1024,2048]{1,0:T(8,128)(2,1)} %get-tuple-element.11) | copy-start | bytes 12582916
  160.6 2.7 %copy-start.15 = (bf16[1024,2048]{1,0:T(8,128)(2,1)S(1)}, bf16[1024,2048]{1,0:T(8,128)(2,1)}, u32[]{:S(2)}) copy-start(bf16[1024,2048]{1,0:T(8,128)(2,1)} %get-tuple-element.10) | copy-start | bytes 12582916
  160.6 2.9 %copy-start.21 = (f32[1024,256]{1,0:T(8,128)S(1)}, f32[1024,256]{1,0:T(8,128)}, u32[]{:S(2)}) copy-start(f32[1024,256]{1,0:T(8,128)} %copy-done.20) | copy-start | bytes 3145732
  160.6 3.5 %copy-start.23 = (f32[1024,256]{1,0:T(8,128)S(1)}, f32[1024,256]{1,0:T(8,128)}, u32[]{:S(2)}) copy-start(f32[1024,256]{1,0:T(8,128)} %copy-done.22) | copy-start | bytes 3145732
  164.1 2.7 %copy-start.10 = (f32[256,256]{1,0:T(8,128)S(1)}, f32[256,256]{1,0:T(8,128)}, u32[]{:S(2)}) copy-start(f32[256,256]{1,0:T(8,128)} %get-tuple-element.18) | copy-start | bytes 786436
  164.1 8.1 %copy-start.8 = (bf16[256,256]{1,0:T(8,128)(2,1)S(1)}, bf16[256,256]{1,0:T(8,128)(2,1)}, u32[]{:S(2)}) copy-start(bf16[256,256]{1,0:T(8,128)(2,1)} %param.17) | copy-start | bytes 393220
  164.1 8.9 %copy-start.9 = (bf16[256,256]{1,0:T(8,128)(2,1)S(1)}, bf16[256,256]{1,0:T(8,128)(2,1)}, u32[]{:S(2)}) copy-start(bf16[256,256]{1,0:T(8,128)(2,1)} %param.18) | copy-start | bytes 393220
  166.8 5.5 %collective-permute-start.1 = (f32[2,256]{1,0:T(2,128)S(1)}, f32[2,256]{1,0:T(2,128)S(1)}, u32[]{:S(2)}, u32[]{:S(2)}) collective-permute-start(f32[2,256]{1,0:T(2,128)S(1)} %slice.60), channel_id=1, source_target_pairs={{4,0},{8,4},{12,8},{16,12},{20,16},{24,20},{28,24},{5,1},{9,5},{13... | collective-permute-start | bytes 6152 | tf_op jit(solution)/shard_map/ppermute | solution.py:16
where the time goes:
time: 183 us
  Pallas kernels  115 us (63%)
  matrix products  28.3 us (15%)
  other arithmetic  11.6 us (6%)
  waiting for transfers between devices  11.5 us (6%)
  starting transfers between devices  10.1 us (6%)
  local copies, waits for them, and re-layouts  5.07 us (3%)
    pallas_call x2, Pallas kernels, gathered(): pl.pallas_call(functools.partial(gather_kernel, n, exchange, count), out_...  82.1 us
    pallas_call x1, Pallas kernels, returned_slots(): pl.pallas_call(functools.partial(return_kernel, n), out_shape=jax.ShapeDt...  32.9 us
    dot_general x5, matrix products, rows_product(): lax.dot_general(left, right, (((0,), (0,)), ((), ())), preferred_element_...  13.1 us
    all_to_all x1, waiting for transfers between devices, shards(): shares = lax.all_to_all(shares, 'sp', split_axis=0, concat_axis=0)  8.04 us
    ppermute x2, starting transfers between devices, passed_along(): lax.ppermute(value, axis, [(source, source + steps) for source in range(f...  6.18 us
    dot_general x3, matrix products, cols_product(): lax.dot_general(left, right, (((1,), (1,)), ((), ())), preferred_element_...  4.15 us
    all_to_all x1, starting transfers between devices, shards(): shares = lax.all_to_all(shares, 'sp', split_axis=0, concat_axis=0)  3.95 us
  transfers between devices with their start and end apart: 3, of which 2 were waited for; matrix products, arithmetic and copies ran while one was open for 20% of the time, Pallas kernels for 63%

commit v1 on v0

v1 whole, which is shorter than its diff:
```python
import functools

import jax
import jax.numpy as jnp
from jax import lax
from jax.experimental import pallas as pl
from jax.experimental.pallas import tpu as pltpu
from jax.sharding import PartitionSpec as P

norm_eps = 1e-06


def passed_along(value, axis, steps):
    count = lax.axis_size(axis)
    first, last = (max(0, -steps), min(count, count - steps))
    return lax.ppermute(value, axis, [(source, source + steps) for source in range(first, last)])


def rows_product(left, right):
    return lax.dot_general(
        left, right, (((0,), (0,)), ((), ())), preferred_element_type=jnp.float32
    )


def cols_product(left, right):
    return lax.dot_general(
        left, right, (((1,), (1,)), ((), ())), preferred_element_type=jnp.float32
    )


MESH = pl.DeviceIdType.MESH


def remote(source, target, send_sem, recv_sem, device):
    return pltpu.make_async_remote_copy(
        src_ref=source,
        dst_ref=target,
        send_sem=send_sem,
        recv_sem=recv_sem,
        device_id=device,
        device_id_type=MESH,
    )


def columns(index, width):
    return pl.ds(pl.multiple_of(index * width, width), width)


def mirrored(me, mask, n):
    found, unit = 0, 1
    while unit < n:
        found = found + lax.rem(lax.div(me, unit) + lax.div(mask, unit), 2) * unit
        unit = 2 * unit
    return found


def tp_places():
    tp, count = lax.axis_index("tp"), lax.axis_size("tp")
    cross = lax.rem(tp + count // 2, count)
    partner = tp + 1 - 2 * lax.rem(tp, 2)
    return (tp, cross, partner, lax.rem(partner + count // 2, count))


def greet(cross, partner):
    barrier = pltpu.get_barrier_semaphore()
    for peer in (cross, partner):
        pl.semaphore_signal(barrier, inc=1, device_id={"tp": peer}, device_id_type=MESH)
    me, n = lax.axis_index("sp"), lax.axis_size("sp")

    def greet_one(k, carry):
        peer = lax.rem(me + k, n)
        pl.semaphore_signal(barrier, inc=1, device_id={"sp": peer}, device_id_type=MESH)
        return carry

    lax.fori_loop(1, n, greet_one, 0)
    return lambda: pl.semaphore_wait(barrier, n + 1)


def loop(low, high, body):
    def step(k, carry):
        body(k)
        return carry

    lax.fori_loop(low, high, step, 0)


def experts_kernel(
    n,
    normed,
    cot,
    route,
    w_gate,
    w_up,
    w_down,
    token,
    rows_out,
    cots_out,
    hidden_out,
    gate_out,
    up_out,
    keys,
    weights,
    arrived,
    arrived_route,
    sending,
    slots,
    hidden,
    gate_grad,
    up_grad,
    partial,
    near,
    far_out,
    far_in,
    total,
    back,
    acc,
    tok_send,
    tok_recv,
    slot_send,
    slot_recv,
    cross_send,
    cross_recv,
    near_send,
    fwd_send,
    near_recv,
    hand_send,
    hand_recv,
    far_send,
    far_recv,
    out_send,
    out_recv,
    all_send,
    all_cross,
    all_near,
    local,
):
    me = lax.axis_index("sp")
    tp, cross, partner, diagonal = tp_places()
    half = n // 2
    count, wide = normed.shape
    width = acc.shape[1]
    depth = near.shape[1] // n
    group = max(1, 256 // depth)
    span = group * depth
    wait_all = greet(cross, partner)
    sources = (normed, cot)

    def other(s):
        return mirrored(me, jnp.int32(s), n)

    def at(s):
        return pl.ds(pl.multiple_of(s * depth, depth), depth)

    def table(which, source):
        c0, c1, s0, s1 = (source[i : i + 1, :] for i in range(4))
        expert = lax.broadcasted_iota(jnp.int32, (n, count), 0).astype(jnp.float32)
        first, second = (c0 == expert, c1 == expert)
        member = jnp.where(first | second, 1.0, 0.0)
        row = lax.broadcasted_iota(jnp.int32, (count, count), 0)
        column = lax.broadcasted_iota(jnp.int32, (count, count), 1)
        before = jnp.where(row < column, 1.0, 0.0).astype(jnp.bfloat16)
        earlier = jnp.dot(
            member.astype(jnp.bfloat16), before, preferred_element_type=jnp.float32
        )
        keys[which] = jnp.where(member > 0.0, earlier, -1.0)
        weights[which] = jnp.where(first, s0, 0.0) + jnp.where(second, s1, 0.0)

    def placing(which, expert):
        slot = lax.broadcasted_iota(jnp.int32, (depth, count), 0).astype(jnp.float32)
        return slot == keys[which, pl.ds(expert, 1), :]

    def chosen(a, which, expert, values):
        mask = placing(which, expert)
        found = jnp.dot(
            jnp.where(mask, 1.0, 0.0).astype(jnp.bfloat16),
            values,
            preferred_element_type=jnp.float32,
        )
        if a == 1:
            weight = jnp.where(mask, weights[which, pl.ds(expert, 1), :], 0.0)
            found = found * jnp.sum(weight, axis=1, keepdims=True)
        return found.astype(jnp.bfloat16)

    def token_copy(a):
        return remote(
            sources[a].at[:, columns(tp, width)],
            arrived.at[a],
            tok_send.at[a],
            tok_recv.at[a],
            {"sp": other(half)},
        )

    def route_copy():
        return remote(route, arrived_route, tok_send.at[2], tok_recv.at[2], {"sp": other(half)})

    def slot_copy(a, s, k):
        return remote(
            sending.at[a, at(s)],
            slots.at[a, at(s), columns(tp, width)],
            slot_send.at[a],
            slot_recv.at[a, s],
            {"sp": other(k)},
        )

    def spread(a, s):
        block = slots.at[a, at(s), columns(tp, width)]
        remote(block, block, cross_send.at[a], cross_recv.at[a, s], {"tp": cross}).start()
        remote(block, block, near_send.at[a], near_recv.at[a, s], {"tp": partner}).start()

    def forward(a, s):
        block = slots.at[a, at(s), columns(cross, width)]
        remote(block, block, cross_send.at[a], cross_recv.at[a, s], {"tp": cross}).wait_recv()
        remote(block, block, fwd_send.at[a], near_recv.at[a, s], {"tp": partner}).start()

    def ready(s):
        for a in (0, 1):
            both = slots.at[a, at(s), pl.ds(0, 2 * width)]
            remote(both, both, near_send.at[a], near_recv.at[a, s], {"tp": partner}).wait_recv()

    def hand(j, s):
        return remote(
            partial.at[at(s), columns((partner, diagonal)[j], width)],
            near.at[j, at(s)],
            hand_send.at[j],
            hand_recv.at[j, s],
            {"tp": partner},
        )

    def across(s):
        return remote(
            far_out.at[at(s)], far_in.at[at(s)], far_send, far_recv.at[s], {"tp": cross}
        )

    def give(s):
        return remote(
            total.at[at(s)], back.at[at(s)], out_send, out_recv.at[s], {"sp": other(s)}
        )

    table(0, route)
    wait_all()
    token_copy(0).start()
    route_copy().start()
    token_copy(1).start()

    def send_own(k):
        for a in (0, 1):
            values = sources[a][:, columns(tp, width)]
            sending[a, at(k), :] = chosen(a, 0, other(k), values)
            slot_copy(a, k, k).start()

    loop(1, half, send_own)
    for a in (0, 1):
        for piece in range(wide // width):
            where = pl.ds(piece * width, width)
            slots[a, pl.ds(0, depth), where] = chosen(a, 0, me, sources[a][:, where])

    def land(s, k):
        for a in (0, 1):
            slot_copy(a, s, k).wait_recv()
            spread(a, s)

    def land_own(k):
        land(k, k)

    loop(1, half, land_own)
    for a in (0, 1):
        if a == 0:
            route_copy().wait_recv()
            table(1, arrived_route)
        token_copy(a).wait_recv()

        def send_other(k):
            sending[a, at(half + k), :] = chosen(a, 1, other(k), arrived[a])
            slot_copy(a, half + k, k).start()

        loop(1, half, send_other)
        slots[a, at(half), columns(tp, width)] = chosen(a, 1, me, arrived[a])
        spread(a, half)

    def forward_both(s):
        for a in (0, 1):
            forward(a, s)

    loop(1, half, forward_both)

    def compute(g):
        rows = pl.ds(pl.multiple_of(g * span, span), span)
        picked, scaled = (slots[0, rows, :], slots[1, rows, :])
        gate_pre = jnp.dot(picked, w_gate[...], preferred_element_type=jnp.float32)
        up_pre = jnp.dot(picked, w_up[...], preferred_element_type=jnp.float32)
        hidden_grad = cols_product(scaled, w_down[...])
        sigmoid_gate = jax.nn.sigmoid(gate_pre)
        silu_gate = gate_pre * sigmoid_gate
        hidden[rows, :] = (silu_gate * up_pre).astype(jnp.bfloat16)
        gate = (
            hidden_grad * up_pre * sigmoid_gate * (1.0 + gate_pre * (1.0 - sigmoid_gate))
        ).astype(jnp.bfloat16)
        up = (hidden_grad * silu_gate).astype(jnp.bfloat16)
        gate_grad[rows, :] = gate
        up_grad[rows, :] = up
        for piece in range(wide // width):
            where = pl.ds(piece * width, width)
            partial[rows, where] = (
                cols_product(gate, w_gate[where, :]) + cols_product(up, w_up[where, :])
            ).astype(jnp.bfloat16)
        for kind, (source, target) in enumerate(kept):
            pltpu.make_async_copy(source.at[rows, :], target.at[rows, :], local.at[kind]).start()

    kept = (
        (slots.at[0], rows_out),
        (slots.at[1], cots_out),
        (hidden, hidden_out),
        (gate_grad, gate_out),
        (up_grad, up_out),
    )

    def work(g):
        def await_one(i):
            s = g * group + i
            @pl.when(s > 0)
            def _():
                ready(s)

        loop(0, group, await_one)
        compute(g)

        def hand_one(i):
            s = g * group + i
            hand(1, s).start()
            hand(0, s).start()

        loop(0, group, hand_one)

    groups = n // group
    loop(0, groups // 2, work)

    def land_other(k):
        land(half + k, k)

        @pl.when(k == 1)
        def _():
            forward_both(half)

        @pl.when(k > 1)
        def _():
            forward_both(half + k - 1)

    loop(1, half, land_other)

    def pair(s):
        hand(1, s).wait_recv()
        mine = partial[at(s), columns(cross, width)].astype(jnp.float32)
        far_out[at(s), :] = (mine + near[1, at(s), :].astype(jnp.float32)).astype(jnp.bfloat16)
        across(s).start()

    loop(0, half, pair)
    forward_both(n - 1)
    loop(groups // 2, groups, work)
    loop(half, n, pair)

    def finish(s):
        hand(0, s).wait_recv()
        across(s).wait_recv()
        mine = partial[at(s), columns(tp, width)].astype(jnp.float32)
        return (
            mine + near[0, at(s), :].astype(jnp.float32) + far_in[at(s), :].astype(jnp.float32)
        ).astype(jnp.bfloat16)

    def finish_one(s):
        total[at(s), :] = finish(s)
        give(s).start()

    loop(1, n, finish_one)
    back[pl.ds(0, depth), :] = finish(0)
    acc[...] = jnp.zeros_like(acc)

    def combine(s):
        @pl.when(s > 0)
        def _():
            give(s).wait_recv()

        mask = jnp.where(placing(0, other(s)), 1.0, 0.0).astype(jnp.bfloat16)
        acc[...] += rows_product(mask, back[at(s), :])

    loop(0, n, combine)
    pieces = all_cross.shape[0]
    tall = count // pieces

    def shared(i, column, send, recv, peer):
        block = token.at[pl.ds(i * tall, tall), columns(column, width)]
        return remote(block, block, send, recv, {"tp": peer})

    token[:, columns(tp, width)] = acc[...].astype(jnp.bfloat16)
    for i in range(pieces):
        shared(i, tp, all_send.at[0, i], all_cross.at[i], cross).start()
        shared(i, tp, all_send.at[1, i], all_near.at[0, i], partner).start()
    for i in range(pieces):
        shared(i, cross, all_send.at[0, i], all_cross.at[i], cross).wait_recv()
        shared(i, cross, all_send.at[2, i], all_near.at[1, i], partner).start()
    for i in range(pieces):
        for j in (0, 1):
            shared(i, tp, all_send.at[j + 1, i], all_near.at[j, i], partner).wait()
        shared(i, tp, all_send.at[0, i], all_cross.at[i], cross).wait_send()
    route_copy().wait_send()
    for a in (0, 1):
        token_copy(a).wait_send()
        sent = sending.at[a, pl.ds(0, (n - 2) * depth)]
        remote(sent, sent, slot_send.at[a], slot_recv.at[a, 0], {"tp": partner}).wait_send()
        most = slots.at[a, pl.ds(0, (n - 1) * depth), pl.ds(0, width)]
        for sem in (cross_send, near_send, fwd_send):
            remote(most, most, sem.at[a], near_recv.at[a, 0], {"tp": partner}).wait_send()
        remote(far_out, far_in, hand_send.at[a], hand_recv.at[a, 0], {"tp": partner}).wait_send()
    remote(far_out, far_in, far_send, far_recv.at[0], {"tp": cross}).wait_send()
    rest = total.at[pl.ds(0, (n - 1) * depth)]
    remote(rest, rest, out_send, out_recv.at[0], {"tp": partner}).wait_send()
    for kind, (source, target) in enumerate(kept):
        pltpu.make_async_copy(source, target, local.at[kind]).wait()


def experts(normed, cot, route, w_gate, w_up, w_down, n):
    count, wide = normed.shape
    hidden = w_gate.shape[1]
    width = wide // lax.axis_size("tp")
    depth = 4 * count // n
    rows = n * depth
    pieces = 2
    kind = normed.dtype

    def out(*shape):
        return jax.ShapeDtypeStruct(shape, kind)

    vmem, anywhere = (pl.BlockSpec(memory_space=pltpu.VMEM), pl.BlockSpec(memory_space=pl.ANY))
    dma = pltpu.SemaphoreType.DMA
    return pl.pallas_call(
        functools.partial(experts_kernel, n),
        out_shape=[
            out(count, wide),
            out(rows, wide),
            out(rows, wide),
            out(rows, hidden),
            out(rows, hidden),
            out(rows, hidden),
        ],
        in_specs=[vmem] * 6,
        out_specs=[vmem] + [anywhere] * 5,
        scratch_shapes=[
            pltpu.VMEM((2, n, count), jnp.float32),
            pltpu.VMEM((2, n, count), jnp.float32),
            pltpu.VMEM((2, count, width), kind),
            pltpu.VMEM(route.shape, jnp.float32),
            pltpu.VMEM((2, rows, width), kind),
            pltpu.VMEM((2, rows, wide), kind),
            pltpu.VMEM((rows, hidden), kind),
            pltpu.VMEM((rows, hidden), kind),
            pltpu.VMEM((rows, hidden), kind),
            pltpu.VMEM((rows, wide), kind),
            pltpu.VMEM((2, rows, width), kind),
            pltpu.VMEM((rows, width), kind),
            pltpu.VMEM((rows, width), kind),
            pltpu.VMEM((rows, width), kind),
            pltpu.VMEM((rows, width), kind),
            pltpu.VMEM((count, width), jnp.float32),
            dma((3,)),
            dma((3,)),
            dma((2,)),
            dma((2, n)),
            dma((2,)),
            dma((2, n)),
            dma((2,)),
            dma((2,)),
            dma((2, n)),
            dma((2,)),
            dma((2, n)),
            dma,
            dma((n,)),
            dma,
            dma((n,)),
            dma((3, pieces)),
            dma((pieces,)),
            dma((2, pieces)),
            dma((5,)),
        ],
        compiler_params=pltpu.CompilerParams(
            collective_id=1, has_side_effects=True, vmem_limit_bytes=52 * 1024 * 1024
        ),
    )(normed, cot, route, w_gate, w_up, w_down)


def shards(
    cotangent,
    stream_in,
    norm_gain,
    out_gate,
    in_gate,
    conv_input,
    conv_taps,
    out_weight,
    expert_gate,
    expert_up,
    expert_down,
    expert_choice,
    route_scale,
):
    sp_size = lax.axis_size("sp")
    tp_size = lax.axis_size("tp")
    rows_here = stream_in.shape[0]
    model_width = stream_in.shape[1]
    column_width = model_width // tp_size
    column_start = lax.axis_index("tp") * column_width
    stream = stream_in.astype(jnp.float32)
    inverse_rms = lax.rsqrt(jnp.mean(stream * stream, axis=-1, keepdims=True) + norm_eps)
    unit_stream = stream * inverse_rms
    normed = (unit_stream * norm_gain).astype(jnp.bfloat16)
    route = jnp.concatenate(
        [expert_choice.T.astype(jnp.float32), route_scale.T, jnp.zeros((4, rows_here), jnp.float32)]
    )
    token_grad, expert_rows, scaled_cot, hidden, gate_grad, up_grad = experts(
        normed, cotangent, route, expert_gate[0], expert_up[0], expert_down[0], sp_size
    )
    grad_down = rows_product(hidden, scaled_cot)[None]
    grad_gate = rows_product(expert_rows, gate_grad)[None]
    grad_up = rows_product(expert_rows, up_grad)[None]
    product = in_gate.astype(jnp.float32) * conv_input.astype(jnp.float32)
    earlier = passed_along(product[-2:], "sp", 1)
    extended = jnp.concatenate([earlier, product], axis=0)
    filtered = conv_taps[0] * product + conv_taps[1] * extended[1:-1] + conv_taps[2] * extended[:-2]
    mixed_in = (out_gate.astype(jnp.float32) * filtered).astype(jnp.bfloat16)
    unit_grad = token_grad.astype(jnp.float32) * norm_gain
    along = jnp.mean(unit_stream * unit_grad, axis=-1, keepdims=True)
    stream_grad = (
        cotangent.astype(jnp.float32) + inverse_rms * (unit_grad - unit_stream * along)
    ).astype(jnp.bfloat16)
    grad_stream = lax.dynamic_slice_in_dim(stream_grad, column_start, column_width, 1)
    mixed_grad = jnp.dot(stream_grad, out_weight, preferred_element_type=jnp.float32)
    grad_out_gate = (mixed_grad * filtered).astype(jnp.bfloat16)
    filtered_grad = mixed_grad * out_gate.astype(jnp.float32)
    later = passed_along(filtered_grad[:2], "sp", -1)
    extended_grad = jnp.concatenate([filtered_grad, later], axis=0)
    product_grad = (
        conv_taps[0] * filtered_grad
        + conv_taps[1] * extended_grad[1:-1]
        + conv_taps[2] * extended_grad[2:]
    )
    grad_in_gate = (product_grad * conv_input.astype(jnp.float32)).astype(jnp.bfloat16)
    grad_conv_input = (product_grad * in_gate.astype(jnp.float32)).astype(jnp.bfloat16)
    shares = rows_product(stream_grad, mixed_in).astype(jnp.bfloat16)
    shares = shares.reshape(sp_size, model_width // sp_size, -1)
    shares = lax.all_to_all(shares, "sp", split_axis=0, concat_axis=0)
    grad_out_weight = jnp.sum(shares.astype(jnp.float32), axis=0)
    return (
        grad_stream,
        grad_out_gate,
        grad_in_gate,
        grad_conv_input,
        grad_out_weight,
        grad_gate,
        grad_up,
        grad_down,
    )


def solution(mesh):
    placed = (
        P("sp", None),
        P("sp", None),
        P(),
        P("sp", "tp"),
        P("sp", "tp"),
        P("sp", "tp"),
        P(None, "tp"),
        P(None, "tp"),
        P("sp", None, "tp"),
        P("sp", None, "tp"),
        P("sp", "tp", None),
        P("sp", None),
        P("sp", None),
    )
    return jax.shard_map(
        shards,
        mesh=mesh,
        in_specs=placed,
        out_specs=(
            P("sp", "tp"),
            P("sp", "tp"),
            P("sp", "tp"),
            P("sp", "tp"),
            P("sp", "tp"),
            P("sp", None, "tp"),
            P("sp", None, "tp"),
            P("sp", "tp", None),
        ),
        check_vma=False,
    )
```

time: 183 us -> 158 us (0.86)
  matrix products: 28.3 us -> 14.2 us
  Pallas kernels: 115 us -> 102 us
  starting transfers between devices: 10.1 us -> 14 us
  local copies, waits for them, and re-layouts: 5.07 us -> 1.83 us
    dot_general x8 -> x0, matrix products: 14 us -> none  [the longest x3 4.15 us: cols_product(): lax.dot_general(left, right, (((1,), (1,)), ((), ())), preferred_element_...]
    pallas_call x3 -> x1, Pallas kernels: 115 us -> 102 us  [experts(): pl.pallas_call(functools.partial(experts_kernel, n), out_shape=[out(count...]
    all_to_all x1, starting transfers between devices: 3.95 us -> 7.87 us  [shards(): shares = lax.all_to_all(shares, 'sp', split_axis=0, concat_axis=0)]
    unnamed x48 -> x24, local copies, waits for them, and re-layouts: 3.49 us -> 0.06 us
    convert_element_type x0 -> x2, other arithmetic: none -> 2.66 us  [the longest x1 1.97 us: shards(): normed = (unit_stream * norm_gain).astype(jnp.bfloat16)]
    dot_general x5 -> x4, matrix products: 13.1 us -> 11.8 us  [rows_product(): lax.dot_general(left, right, (((0,), (0,)), ((), ())), preferred_element_...]
  transfers between devices with their start and end apart: 3 -> 3, of which waited for: 2 -> 2; matrix products, arithmetic and copies ran while one was open for 20% -> 14% of each run, Pallas kernels for 63% -> 65%
where the time goes in v1:
time: 158 us
  Pallas kernels  102 us (65%)
  matrix products  14.2 us (9%)
  starting transfers between devices  14 us (9%)
  other arithmetic  12.6 us (8%)
  waiting for transfers between devices  12.4 us (8%)
  local copies, waits for them, and re-layouts  1.83 us (1%)
    pallas_call x1, Pallas kernels, experts(): pl.pallas_call(functools.partial(experts_kernel, n), out_shape=[out(count...  102 us
    dot_general x4, matrix products, rows_product(): lax.dot_general(left, right, (((0,), (0,)), ((), ())), preferred_element_...  11.8 us
    all_to_all x1, waiting for transfers between devices, shards(): shares = lax.all_to_all(shares, 'sp', split_axis=0, concat_axis=0)  9.86 us
    all_to_all x1, starting transfers between devices, shards(): shares = lax.all_to_all(shares, 'sp', split_axis=0, concat_axis=0)  7.87 us
    ppermute x2, starting transfers between devices, passed_along(): lax.ppermute(value, axis, [(source, source + steps) for source in range(f...  6.18 us
  transfers between devices with their start and end apart: 3, of which 2 were waited for; matrix products, arithmetic and copies ran while one was open for 14% of the time, Pallas kernels for 65%

profile of v1, /device:TPU:0, one launch (start us, length us, event | category | flops | bytes accessed | tf_op | source)
XLA Modules:
  0.0 157.9 jit_solution(10655449613808553924)
XLA Ops:
  0.6 0.0 copy-start
  0.6 0.0 copy-start.1
  0.7 0.0 copy-start.10
  0.7 1.1 convert_multiply_fusion.6
  1.8 4.9 %collective-permute-start = (f32[2,256]{1,0:T(2,128)S(1)}, f32[2,256]{1,0:T(2,128)S(1)}, u32[]{:S(2)}, u32[]{:S(2)}) collective-permute-start(f32[2,256]{1,0:T(2,128)S(1)} %slice.39), channel_id=1, source_target_pairs={{0,4},{4,8},{8,12},{12,16},{16,20},{20,24},{24,28},{1,5},{5,9},{9,... | collective-permute-start | bytes 6152 | tf_op jit(solution)/shard_map/ppermute | solution.py:16
  6.7 1.5 fusion.9
  8.3 0.7 convert_bitcast_fusion
  8.9 0.1 pad.6.clone
  9.0 0.0 copy-done.1
  9.0 2.0 %fusion.3.normed = bf16[256,2048]{1,0:T(8,128)(2,1)} fusion(bf16[256,2048]{1,0:T(8,128)(2,1)S(1)} %copy-done.1, f32[2048]{0:T(1024)} %param.15, f32[256]{0:T(256)S(1)} %add_rsqrt_fusion), kind=kLoop, calls=%fused_computation.9 | loop fusion | flops 2097152 | bytes 2106368 | tf_op jit(solution)/shard_map/convert_element_type | solution.py:513
  11.0 0.0 copy-done.10
  11.0 0.1 maximum_maximum_fusion.route
  11.1 0.0 copy-start.8
  11.1 102.1 %shard_map.188 = (bf16[256,2048]{1,0:T(8,128)(2,1)}, bf16[1024,2048]{1,0:T(8,128)(2,1)}, bf16[1024,2048]{1,0:T(8,128)(2,1)}, bf16[1024,256]{1,0:T(8,128)(2,1)S(1...) custom-call(bf16[256,2048]{1,0:T(8,128)(2,1)} %fusion.3.normed, bf16[256,2048]{1,0:T(8,128)(2,1)} %cot.1, ...), custom_call_target="tpu_custom_call" | custom-call | tf_op jit(solution)/shard_map/pallas_call | solution.py:434
  113.2 0.0 copy-start.3
  113.2 0.0 copy-start.4
  113.2 0.0 copy-done.8
  113.2 1.9 %fusion.4 = f32[256]{0:T(256)S(1)} fusion(bf16[256,2048]{1,0:T(8,128)(2,1)S(1)} %copy-done.1, bf16[256,2048]{1,0:T(8,128)(2,1)} %get-tuple-element.14, f32[2048]{0:T(1024)S(1)} %copy-done.8, f32[256]{0:T(256)S(1)} %add_rsqrt_fusion), kind=kLoop, calls=%fused_computation.10 | loop fusion | flops 3145472 | bytes 2107392 | tf_op jit(solution)/shard_map/reduce_sum | solution.py:529
  115.1 0.0 copy-done.3
  115.1 0.0 copy-done.4
  115.1 0.0 copy-start.9
  115.2 0.0 copy-start.7
  115.2 1.7 %fusion.8 = bf16[256,2048]{1,0:T(8,128)(2,1)} fusion(bf16[256,2048]{1,0:T(8,128)(2,1)S(1)} %copy-done.1, bf16[256,2048]{1,0:T(8,128)(2,1)S(1)} %copy-done.4, bf16[256,2048]{1,0:T(8,128)(2,1)S(1)} %copy-done.3, f32[256]{0:T(256)S(1)} %broadcast_multiply_fusion, f32[2048]{0:T(1024)S(1)} %copy-done.8, f32[256]{0:T(256)S(1)} %add_rsqrt_fusion), kind=kLoop, calls=%fused_computation.14 | loop fusion | flops 5242880 | bytes 4204544 | tf_op jit(solution)/shard_map/convert_element_type | solution.py:532
  116.9 0.0 copy-done.9
  116.9 0.0 copy-start.2
  116.9 0.0 collective-permute-done
  116.9 0.0 copy-done
  116.9 0.0 copy-done.7
  116.9 2.4 %multiply_convert_fusion = (bf16[256,256]{1,0:T(8,128)(2,1)}, f32[256,256]{1,0:T(8,128)S(1)}, f32[256,256]{1,0:T(8,128)S(1)}) fusion(f32[256,256]{1,0:T(8,128)S(1)} %convert_multiply_fusion.6, f32[2,256]{1,0:T(2,128)S(1)} %collective-permute-done, f32[256]{0:T(256)S(1)} %bitcast.31, f32[256]{0:T(256)S(1)} %bitcast.33, f32[256]{0:T(256)S(1)} %bitcast.29, ...), kind=kOutput, calls=%fused_computation.42 | convolution fusion | flops 269156352 | bytes 3150848 | tf_op jit(solution)/shard_map/dot_general | solution.py:534
  119.3 0.0 copy-done.2
  119.4 1.5 convolution_convert_fusion
  120.8 7.9 %all-to-all-start = ((bf16[8,256,256]{2,1,0:T(8,128)(2,1)}), bf16[8,256,256]{2,1,0:T(8,128)(2,1)}, u32[]{:S(2)}, u32[]{:S(2)}) async-start(bf16[8,256,256]{2,1,0:T(8,128)(2,1)} %bitcast.25), calls=%async_computation | async-start | bytes 2097152 | tf_op jit(solution)/shard_map/all_to_all | solution.py:548
  128.7 0.0 copy-start.11
  128.7 4.9 %convolution_bitcast_fusion = f32[1,256,2048]{2,1,0:T(8,128)} fusion(bf16[1024,256]{1,0:T(8,128)(2,1)S(1)} %get-tuple-element.18, bf16[1024,2048]{1,0:T(8,128)(2,1)} %get-tuple-element.19), kind=kOutput, calls=%fused_computation | convolution fusion | flops 1073741824 | bytes 6815744 | tf_op jit(solution)/shard_map/dot_general | solution.py:20
  133.6 0.0 copy-done.11
  133.6 2.7 %convolution_bitcast_fusion.2 = f32[1,2048,256]{2,1,0:T(8,128)} fusion(bf16[1024,2048]{1,0:T(8,128)(2,1)S(1)} %copy-done.11, bf16[1024,256]{1,0:T(8,128)(2,1)S(1)} %get-tuple-element.16), kind=kOutput, calls=%fused_computation.2 | convolution fusion | flops 1073741824 | bytes 6815744 | tf_op jit(solution)/shard_map/dot_general | solution.py:20
  136.3 0.0 copy-start.5
  136.3 0.0 copy-start.6
  136.3 2.7 %convolution_bitcast_fusion.1 = f32[1,2048,256]{2,1,0:T(8,128)} fusion(bf16[1024,2048]{1,0:T(8,128)(2,1)S(1)} %copy-done.11, bf16[1024,256]{1,0:T(8,128)(2,1)S(1)} %get-tuple-element.17), kind=kOutput, calls=%fused_computation.1 | convolution fusion | flops 1073741824 | bytes 6815744 | tf_op jit(solution)/shard_map/dot_general | solution.py:20
  139.0 1.3 collective-permute-start.1
  140.3 1.7 %constant_dynamic-slice_fusion = bf16[256,512]{1,0:T(8,128)(2,1)} fusion(bf16[256,2048]{1,0:T(8,128)(2,1)} %fusion.8, s32[]{:T(128)S(6)} %select_n.3), kind=kLoop, calls=%fused_computation.47 | loop fusion | bytes 524292 | tf_op jit(solution)/shard_map/dynamic_slice | solution.py:533
  142.0 2.5 %collective-permute-done.1 = f32[2,256]{1,0:T(2,128)S(1)} collective-permute-done((f32[2,256]{1,0:T(2,128)S(1)}, f32[2,256]{1,0:T(2,128)S(1)}, u32[]{:S(2)}, u32[]{:S(2)}) %collective-permute-start.1) | collective-permute-done | bytes 2080 | tf_op jit(solution)/shard_map/ppermute | solution.py:16
  144.5 0.0 copy-done.5
  144.5 0.8 fusion.18
  145.2 0.0 copy-done.6
  145.2 0.7 fusion.19
  145.9 9.9 %all-to-all-done = bf16[8,256,256]{2,1,0:T(8,128)(2,1)} async-done(((bf16[8,256,256]{2,1,0:T(8,128)(2,1)}), bf16[8,256,256]{2,1,0:T(8,128)(2,1)}, u32[]{:S(2)}, u32[]{:S(2)}) %all-to-all-start) | async-done | bytes 1048608 | tf_op jit(solution)/shard_map/all_to_all | solution.py:548
  155.8 2.1 %convert_reduce_fusion = f32[256,256]{1,0:T(8,128)} fusion(bf16[8,256,256]{2,1,0:T(8,128)(2,1)} %all-to-all-done), kind=kLoop, calls=%fused_computation.16 | loop fusion | flops 983040 | bytes 1310720 | tf_op jit(solution)/shard_map/reduce_sum | solution.py:549
  (6 shorter events, 0.0 us)
Async XLA Ops:
  0.6 116.3 %copy-start = (bf16[2048,256]{1,0:T(8,128)(2,1)S(1)}, bf16[2048,256]{1,0:T(8,128)(2,1)}, u32[]{:S(2)}) copy-start(bf16[2048,256]{1,0:T(8,128)(2,1)} %param.20) | copy-start | bytes 3145732
  0.6 8.4 %copy-start.1 = (bf16[256,2048]{1,0:T(8,128)(2,1)S(1)}, bf16[256,2048]{1,0:T(8,128)(2,1)}, u32[]{:S(2)}) copy-start(bf16[256,2048]{1,0:T(8,128)(2,1)} %param.14) | copy-start | bytes 3145732
  0.7 10.3 %copy-start.10 = (f32[256,2]{0,1:T(2,128)S(1)}, f32[256,2]{0,1:T(2,128)}, u32[]{:S(2)}) copy-start(f32[256,2]{0,1:T(2,128)} %param.25) | copy-start | bytes 6148
  1.8 115.1 %collective-permute-start = (f32[2,256]{1,0:T(2,128)S(1)}, f32[2,256]{1,0:T(2,128)S(1)}, u32[]{:S(2)}, u32[]{:S(2)}) collective-permute-start(f32[2,256]{1,0:T(2,128)S(1)} %slice.39), channel_id=1, source_target_pairs={{0,4},{4,8},{8,12},{12,16},{16,20},{20,24},{24,28},{1,5},{5,9},{9,... | collective-permute-start | bytes 6152 | tf_op jit(solution)/shard_map/ppermute | solution.py:16
  11.1 102.1 %copy-start.8 = (f32[2048]{0:T(1024)S(1)}, f32[2048]{0:T(1024)}, u32[]{:S(2)}) copy-start(f32[2048]{0:T(1024)} %param.15) | copy-start | bytes 24580
  113.2 2.0 %copy-start.3 = (bf16[256,2048]{1,0:T(8,128)(2,1)S(1)}, bf16[256,2048]{1,0:T(8,128)(2,1)}, u32[]{:S(2)}) copy-start(bf16[256,2048]{1,0:T(8,128)(2,1)} %cot.1) | copy-start | bytes 3145732
  113.2 2.0 %copy-start.4 = (bf16[256,2048]{1,0:T(8,128)(2,1)S(1)}, bf16[256,2048]{1,0:T(8,128)(2,1)}, u32[]{:S(2)}) copy-start(bf16[256,2048]{1,0:T(8,128)(2,1)} %get-tuple-element.14) | copy-start | bytes 3145732
  115.1 1.8 %copy-start.9 = (f32[3,256]{1,0:T(4,128)S(1)}, f32[3,256]{1,0:T(4,128)}, u32[]{:S(2)}) copy-start(f32[3,256]{1,0:T(4,128)} %param.19) | copy-start | bytes 9220
  115.2 1.8 %copy-start.7 = (bf16[256,256]{1,0:T(8,128)(2,1)S(1)}, bf16[256,256]{1,0:T(8,128)(2,1)}, u32[]{:S(2)}) copy-start(bf16[256,256]{1,0:T(8,128)(2,1)} %param.16) | copy-start | bytes 393220
  116.9 2.4 %copy-start.2 = (bf16[256,2048]{1,0:T(8,128)(2,1)S(1)}, bf16[256,2048]{1,0:T(8,128)(2,1)}, u32[]{:S(2)}) copy-start(bf16[256,2048]{1,0:T(8,128)(2,1)} %fusion.8) | copy-start | bytes 3145732
  120.8 34.9 %all-to-all-start = ((bf16[8,256,256]{2,1,0:T(8,128)(2,1)}), bf16[8,256,256]{2,1,0:T(8,128)(2,1)}, u32[]{:S(2)}, u32[]{:S(2)}) async-start(bf16[8,256,256]{2,1,0:T(8,128)(2,1)} %bitcast.25), calls=%async_computation | async-start | bytes 2097152 | tf_op jit(solution)/shard_map/all_to_all | solution.py:548
  128.7 4.9 %copy-start.11 = (bf16[1024,2048]{1,0:T(8,128)(2,1)S(1)}, bf16[1024,2048]{1,0:T(8,128)(2,1)}, u32[]{:S(2)}) copy-start(bf16[1024,2048]{1,0:T(8,128)(2,1)} %get-tuple-element.15) | copy-start | bytes 12582916
  136.3 8.2 %copy-start.5 = (bf16[256,256]{1,0:T(8,128)(2,1)S(1)}, bf16[256,256]{1,0:T(8,128)(2,1)}, u32[]{:S(2)}) copy-start(bf16[256,256]{1,0:T(8,128)(2,1)} %param.17) | copy-start | bytes 393220
  136.3 8.9 %copy-start.6 = (bf16[256,256]{1,0:T(8,128)(2,1)S(1)}, bf16[256,256]{1,0:T(8,128)(2,1)}, u32[]{:S(2)}) copy-start(bf16[256,256]{1,0:T(8,128)(2,1)} %param.18) | copy-start | bytes 393220
  139.0 5.5 %collective-permute-start.1 = (f32[2,256]{1,0:T(2,128)S(1)}, f32[2,256]{1,0:T(2,128)S(1)}, u32[]{:S(2)}, u32[]{:S(2)}) collective-permute-start(f32[2,256]{1,0:T(2,128)S(1)} %slice.42), channel_id=1, source_target_pairs={{4,0},{8,4},{12,8},{16,12},{20,16},{24,20},{28,24},{5,1},{9,5},{13... | collective-permute-start | bytes 6152 | tf_op jit(solution)/shard_map/ppermute | solution.py:16

commit v2 on v1

v2 whole, which is shorter than its diff:
```python
import functools

import jax
import jax.numpy as jnp
from jax import lax
from jax.experimental import pallas as pl
from jax.experimental.pallas import tpu as pltpu
from jax.sharding import PartitionSpec as P

norm_eps = 1e-06


def rows_product(left, right):
    return lax.dot_general(
        left, right, (((0,), (0,)), ((), ())), preferred_element_type=jnp.float32
    )


def cols_product(left, right):
    return lax.dot_general(
        left, right, (((1,), (1,)), ((), ())), preferred_element_type=jnp.float32
    )


MESH = pl.DeviceIdType.MESH


def remote(source, target, send_sem, recv_sem, device):
    return pltpu.make_async_remote_copy(
        src_ref=source,
        dst_ref=target,
        send_sem=send_sem,
        recv_sem=recv_sem,
        device_id=device,
        device_id_type=MESH,
    )


def columns(index, width):
    return pl.ds(pl.multiple_of(index * width, width), width)


def mirrored(me, mask, n):
    found, unit = 0, 1
    while unit < n:
        found = found + lax.rem(lax.div(me, unit) + lax.div(mask, unit), 2) * unit
        unit = 2 * unit
    return found


def tp_places():
    tp, count = lax.axis_index("tp"), lax.axis_size("tp")
    cross = lax.rem(tp + count // 2, count)
    partner = tp + 1 - 2 * lax.rem(tp, 2)
    return (tp, cross, partner, lax.rem(partner + count // 2, count))


def greet(cross, partner):
    barrier = pltpu.get_barrier_semaphore()
    for peer in (cross, partner):
        pl.semaphore_signal(barrier, inc=1, device_id={"tp": peer}, device_id_type=MESH)
    me, n = lax.axis_index("sp"), lax.axis_size("sp")

    def greet_one(k, carry):
        peer = lax.rem(me + k, n)
        pl.semaphore_signal(barrier, inc=1, device_id={"sp": peer}, device_id_type=MESH)
        return carry

    lax.fori_loop(1, n, greet_one, 0)
    return lambda: pl.semaphore_wait(barrier, n + 1)


def loop(low, high, body):
    def step(k, carry):
        body(k)
        return carry

    lax.fori_loop(low, high, step, 0)


def step_kernel(
    n,
    stream,
    cot,
    gain,
    route,
    out_gate,
    in_gate,
    conv_input,
    taps,
    w_out_hbm,
    w_gate_hbm,
    w_up_hbm,
    w_down_hbm,
    stream_out,
    out_gate_out,
    in_gate_out,
    conv_input_out,
    w_out_grad,
    gate_out,
    up_out,
    down_out,
    normed,
    inverse,
    along,
    w_out,
    w_gate,
    w_up,
    w_down,
    keys,
    weights,
    arrived,
    arrived_route,
    sending,
    slots,
    hidden,
    both_grad,
    partial,
    near,
    far_out,
    far_in,
    total,
    back,
    acc,
    token,
    extended,
    filtered,
    extended_grad,
    mixed,
    stream_grad,
    turned,
    turned_all,
    gate_sum,
    up_sum,
    down_sum,
    small,
    w_out_sum,
    load,
    tok_send,
    tok_recv,
    slot_send,
    slot_recv,
    cross_send,
    cross_recv,
    near_send,
    fwd_send,
    near_recv,
    hand_send,
    hand_recv,
    far_send,
    far_recv,
    out_send,
    out_recv,
    all_send,
    all_cross,
    all_near,
    halo_send,
    halo_recv,
    mix_send,
    mix_recv,
    turn_send,
    turn_recv,
    turn_cross,
    turn_near,
    local,
):
    me = lax.axis_index("sp")
    tp, cross, partner, diagonal = tp_places()
    half = n // 2
    count, wide = normed.shape
    width = acc.shape[1]
    depth = near.shape[1] // n
    group = max(1, 256 // depth)
    span = group * depth
    chunk = min(256, width)
    channels = filtered.shape[1]
    block = wide // n
    shared_parts = wide // width
    shared_parts = shared_parts if block % (16 * shared_parts) == 0 else 1
    share = block // shared_parts
    wait_all = greet(cross, partner)
    sources = (normed, cot)
    loads = [
        pltpu.make_async_copy(source, target, load.at[i])
        for i, (source, target) in enumerate(
            ((w_gate_hbm, w_gate), (w_up_hbm, w_up), (w_down_hbm, w_down), (w_out_hbm, w_out))
        )
    ]
    for one in loads:
        one.start()

    def other(s):
        return mirrored(me, jnp.int32(s), n)

    def at(s):
        return pl.ds(pl.multiple_of(s * depth, depth), depth)

    def normalize(i):
        rows = pl.ds(pl.multiple_of(i * 32, 32), 32)
        values = stream[rows, :].astype(jnp.float32)
        scale = lax.rsqrt(jnp.mean(values * values, axis=-1, keepdims=True) + norm_eps)
        inverse[rows, :] = scale
        normed[rows, :] = (values * scale * gain[...]).astype(jnp.bfloat16)

    def table(which, source):
        c0, c1, s0, s1 = (source[i : i + 1, :] for i in range(4))
        expert = lax.broadcasted_iota(jnp.int32, (n, count), 0).astype(jnp.float32)
        first, second = (c0 == expert, c1 == expert)
        member = jnp.where(first | second, 1.0, 0.0)
        row = lax.broadcasted_iota(jnp.int32, (count, count), 0)
        column = lax.broadcasted_iota(jnp.int32, (count, count), 1)
        before = jnp.where(row < column, 1.0, 0.0).astype(jnp.bfloat16)
        earlier = jnp.dot(
            member.astype(jnp.bfloat16), before, preferred_element_type=jnp.float32
        )
        keys[which] = jnp.where(member > 0.0, earlier, -1.0)
        weights[which] = jnp.where(first, s0, 0.0) + jnp.where(second, s1, 0.0)

    def placing(which, expert):
        slot = lax.broadcasted_iota(jnp.int32, (depth, count), 0).astype(jnp.float32)
        return slot == keys[which, pl.ds(expert, 1), :]

    def chosen(a, which, expert, values):
        mask = placing(which, expert)
        found = jnp.dot(
            jnp.where(mask, 1.0, 0.0).astype(jnp.bfloat16),
            values,
            preferred_element_type=jnp.float32,
        )
        if a == 1:
            weight = jnp.where(mask, weights[which, pl.ds(expert, 1), :], 0.0)
            found = found * jnp.sum(weight, axis=1, keepdims=True)
        return found.astype(jnp.bfloat16)

    def token_copy(a):
        return remote(
            sources[a].at[:, columns(tp, width)],
            arrived.at[a],
            tok_send.at[a],
            tok_recv.at[a],
            {"sp": other(half)},
        )

    def route_copy():
        return remote(route, arrived_route, tok_send.at[2], tok_recv.at[2], {"sp": other(half)})

    def slot_copy(a, s, k):
        return remote(
            sending.at[a, at(s)],
            slots.at[a, at(s), columns(tp, width)],
            slot_send.at[a],
            slot_recv.at[a, s],
            {"sp": other(k)},
        )

    def spread(a, s):
        part = slots.at[a, at(s), columns(tp, width)]
        remote(part, part, cross_send.at[a], cross_recv.at[a, s], {"tp": cross}).start()
        remote(part, part, near_send.at[a], near_recv.at[a, s], {"tp": partner}).start()

    def forward(a, s):
        part = slots.at[a, at(s), columns(cross, width)]
        remote(part, part, cross_send.at[a], cross_recv.at[a, s], {"tp": cross}).wait_recv()
        remote(part, part, fwd_send.at[a], near_recv.at[a, s], {"tp": partner}).start()

    def ready(s):
        for a in (0, 1):
            both = slots.at[a, at(s), pl.ds(0, 2 * width)]
            remote(both, both, near_send.at[a], near_recv.at[a, s], {"tp": partner}).wait_recv()

    def hand(j, s):
        return remote(
            partial.at[at(s), columns((partner, diagonal)[j], width)],
            near.at[j, at(s)],
            hand_send.at[j],
            hand_recv.at[j, s],
            {"tp": partner},
        )

    def across(s):
        return remote(
            far_out.at[at(s)], far_in.at[at(s)], far_send, far_recv.at[s], {"tp": cross}
        )

    def give(s):
        return remote(
            total.at[at(s)], back.at[at(s)], out_send, out_recv.at[s], {"sp": other(s)}
        )

    def halo_later():
        peer = lax.rem(me + 1, n)
        return remote(
            extended.at[pl.ds(count, 8)],
            extended.at[pl.ds(0, 8)],
            halo_send.at[0],
            halo_recv.at[0],
            {"sp": peer},
        )

    def halo_earlier():
        peer = lax.rem(me + n - 1, n)
        return remote(
            extended_grad.at[pl.ds(0, 8)],
            extended_grad.at[pl.ds(count, 8)],
            halo_send.at[1],
            halo_recv.at[1],
            {"sp": peer},
        )

    def mix_copy(source, target, k):
        return remote(
            mixed.at[source], mixed.at[target], mix_send, mix_recv.at[target], {"sp": other(k)}
        )

    with jax.named_scope("prep"):
        loop(0, count // 32, normalize)
        table(0, route)
        product = in_gate[...].astype(jnp.float32) * conv_input[...].astype(jnp.float32)
        extended[pl.ds(8, count), :] = product

        @pl.when(me == 0)
        def _():
            extended[pl.ds(0, 8), :] = jnp.zeros((8, channels), jnp.float32)

        @pl.when(me == n - 1)
        def _():
            extended_grad[pl.ds(count, 8), :] = jnp.zeros((8, channels), jnp.float32)

    with jax.named_scope("barrier"):
        wait_all()

    def send_own(k):
        for a in (0, 1):
            values = sources[a][:, columns(tp, width)]
            sending[a, at(k), :] = chosen(a, 0, other(k), values)
            slot_copy(a, k, k).start()

    with jax.named_scope("send_own"):
        loop(1, half, send_own)
        token_copy(0).start()
        route_copy().start()
        token_copy(1).start()

        @pl.when(me < n - 1)
        def _():
            halo_later().start()

    with jax.named_scope("own_block"):
        for a in (0, 1):
            for piece in range(wide // width):
                where = pl.ds(piece * width, width)
                slots[a, pl.ds(0, depth), where] = chosen(a, 0, me, sources[a][:, where])

    def land(s, k):
        for a in (0, 1):
            slot_copy(a, s, k).wait_recv()
            spread(a, s)

    def land_own(k):
        land(k, k)

    with jax.named_scope("land_own"):
        loop(1, half, land_own)

    with jax.named_scope("filter"):
        @pl.when(me > 0)
        def _():
            halo_later().wait_recv()

        filtered[...] = (
            taps[0:1, :] * extended[pl.ds(8, count), :]
            + taps[1:2, :] * extended[pl.ds(7, count), :]
            + taps[2:3, :] * extended[pl.ds(6, count), :]
        )
        mixed[0] = (out_gate[...].astype(jnp.float32) * filtered[...]).astype(jnp.bfloat16)

    for a in (0, 1):
        with jax.named_scope("await_tokens"):
            if a == 0:
                route_copy().wait_recv()
                table(1, arrived_route)
            token_copy(a).wait_recv()

        def send_other(k):
            sending[a, at(half + k), :] = chosen(a, 1, other(k), arrived[a])
            slot_copy(a, half + k, k).start()

        with jax.named_scope("send_other"):
            loop(1, half, send_other)
            slots[a, at(half), columns(tp, width)] = chosen(a, 1, me, arrived[a])
            spread(a, half)

    def forward_both(s):
        for a in (0, 1):
            forward(a, s)

    with jax.named_scope("forward_own"):
        mix_copy(0, half, half).start()

        def mix_own(k):
            mix_copy(0, k, k).start()

        loop(1, half, mix_own)
        loop(1, half, forward_both)

    def compute(g):
        rows = pl.ds(pl.multiple_of(g * span, span), span)
        picked, scaled = (slots[0, rows, :], slots[1, rows, :])
        gate_pre = jnp.dot(picked, w_gate[...], preferred_element_type=jnp.float32)
        up_pre = jnp.dot(picked, w_up[...], preferred_element_type=jnp.float32)
        hidden_grad = cols_product(scaled, w_down[...])
        sigmoid_gate = jax.nn.sigmoid(gate_pre)
        silu_gate = gate_pre * sigmoid_gate
        hidden[rows, :] = (silu_gate * up_pre).astype(jnp.bfloat16)
        gate = (
            hidden_grad * up_pre * sigmoid_gate * (1.0 + gate_pre * (1.0 - sigmoid_gate))
        ).astype(jnp.bfloat16)
        up = (hidden_grad * silu_gate).astype(jnp.bfloat16)
        across_hidden = gate.shape[1]
        both_grad[rows, pl.ds(0, across_hidden)] = gate
        both_grad[rows, pl.ds(across_hidden, across_hidden)] = up
        for piece in range(wide // width):
            where = pl.ds(piece * width, width)
            partial[rows, where] = (
                cols_product(gate, w_gate[where, :]) + cols_product(up, w_up[where, :])
            ).astype(jnp.bfloat16)

    def work(g):
        def await_one(i):
            s = g * group + i

            @pl.when(s > 0)
            def _():
                ready(s)

        loop(0, group, await_one)
        compute(g)

        def hand_one(i):
            s = g * group + i
            hand(1, s).start()
            hand(0, s).start()

        loop(0, group, hand_one)

    groups = n // group
    with jax.named_scope("work_own"):
        for i in range(3):
            loads[i].wait()
        loop(0, groups // 2, work)

    def land_other(k):
        land(half + k, k)

        @pl.when(k == 1)
        def _():
            forward_both(half)

        @pl.when(k > 1)
        def _():
            forward_both(half + k - 1)

    with jax.named_scope("land_other"):
        loop(1, half, land_other)

    def pair(s):
        hand(1, s).wait_recv()
        mine = partial[at(s), columns(cross, width)].astype(jnp.float32)
        far_out[at(s), :] = (mine + near[1, at(s), :].astype(jnp.float32)).astype(jnp.bfloat16)
        across(s).start()

    with jax.named_scope("pair_own"):
        loop(0, half, pair)
        mix_copy(half, half, half).wait_recv()

        def mix_other(k):
            mix_copy(half, half + k, k).start()

        loop(1, half, mix_other)
    with jax.named_scope("forward_last"):
        forward_both(n - 1)
    with jax.named_scope("work_other"):
        loop(groups // 2, groups, work)
    with jax.named_scope("pair_other"):
        loop(half, n, pair)

    def finish(s):
        hand(0, s).wait_recv()
        across(s).wait_recv()
        mine = partial[at(s), columns(tp, width)].astype(jnp.float32)
        return (
            mine + near[0, at(s), :].astype(jnp.float32) + far_in[at(s), :].astype(jnp.float32)
        ).astype(jnp.bfloat16)

    def finish_one(s):
        total[at(s), :] = finish(s)
        give(s).start()

    def grad_copies(c):
        rows = pl.ds(pl.multiple_of(c * chunk, chunk), chunk)
        return [
            pltpu.make_async_copy(source, target, local.at[i])
            for i, (source, target) in enumerate(
                (
                    (gate_sum.at[rows, :], gate_out.at[rows, :]),
                    (up_sum.at[rows, :], up_out.at[rows, :]),
                    (down_sum.at[:, rows], down_out.at[:, rows]),
                )
            )
        ]

    def grads(c):
        rows = pl.ds(pl.multiple_of(c * chunk, chunk), chunk)
        sums = rows_product(slots[0, :, rows], both_grad[...])
        gate_sum[rows, :] = sums[:, : sums.shape[1] // 2]
        up_sum[rows, :] = sums[:, sums.shape[1] // 2 :]
        down_sum[:, rows] = rows_product(hidden[...], slots[1, :, rows])
        for one in grad_copies(c):
            one.start()

    with jax.named_scope("finish_own"):
        loop(1, half, finish_one)
        back[pl.ds(0, depth), :] = finish(0)
    with jax.named_scope("grads"):
        loop(0, wide // chunk // 2, grads)
    with jax.named_scope("finish_other"):
        loop(half, n, finish_one)
    with jax.named_scope("grads"):
        loop(wide // chunk // 2, wide // chunk, grads)
    acc[...] = jnp.zeros_like(acc)

    def combine(s):
        @pl.when(s > 0)
        def _():
            give(s).wait_recv()

        mask = jnp.where(placing(0, other(s)), 1.0, 0.0).astype(jnp.bfloat16)
        acc[...] += rows_product(mask, back[at(s), :])

    with jax.named_scope("combine"):
        loop(0, n, combine)
    pieces = all_cross.shape[0]
    tall = count // pieces

    def shared(i, column, send, recv, peer):
        part = token.at[pl.ds(i * tall, tall), columns(column, width)]
        return remote(part, part, send, recv, {"tp": peer})

    with jax.named_scope("share"):
        token[:, columns(tp, width)] = acc[...].astype(jnp.bfloat16)
        for i in range(pieces):
            shared(i, tp, all_send.at[0, i], all_cross.at[i], cross).start()
            shared(i, tp, all_send.at[1, i], all_near.at[0, i], partner).start()
        for i in range(pieces):
            shared(i, cross, all_send.at[0, i], all_cross.at[i], cross).wait_recv()
            shared(i, cross, all_send.at[2, i], all_near.at[1, i], partner).start()
        for i in range(pieces):
            for j in (0, 1):
                shared(i, tp, all_send.at[j + 1, i], all_near.at[j, i], partner).wait()
            shared(i, tp, all_send.at[0, i], all_cross.at[i], cross).wait_send()

    def reduce_along(i):
        rows = pl.ds(pl.multiple_of(i * 32, 32), 32)
        unit = stream[rows, :].astype(jnp.float32) * inverse[rows, :]
        unit_grad = token[rows, :].astype(jnp.float32) * gain[...]
        along[rows, :] = jnp.mean(unit * unit_grad, axis=-1, keepdims=True)

    def total_grad(c):
        where = pl.ds(pl.multiple_of(c * chunk, chunk), chunk)
        scale = inverse[...]
        unit = stream[:, where].astype(jnp.float32) * scale
        unit_grad = token[:, where].astype(jnp.float32) * gain[:, where]
        value = cot[:, where].astype(jnp.float32) + scale * (unit_grad - unit * along[...])
        value = value.astype(jnp.bfloat16)
        stream_grad[:, where] = value
        turned[where, :] = jnp.transpose(value.astype(jnp.float32)).astype(jnp.bfloat16)

    with jax.named_scope("stream_grad"):
        loop(0, count // 32, reduce_along)
        loop(0, wide // chunk, total_grad)

    def turned_rows(owner, part):
        return pl.ds(pl.multiple_of(owner * block + part * share, share), share)

    def part_rows(part):
        return pl.ds(pl.multiple_of(part * share, share), share)

    mine_part = tp if shared_parts > 1 else 0
    cross_part = cross if shared_parts > 1 else 0

    def turn_copy(s):
        return remote(
            turned.at[turned_rows(other(s), mine_part)],
            turned_all.at[s, part_rows(mine_part)],
            turn_send.at[0],
            turn_recv.at[s],
            {"sp": other(s)},
        )

    def turn_part(s, part, send, recv, peer):
        rows = turned_all.at[s, part_rows(part)]
        return remote(rows, rows, send, recv, {"tp": peer})

    def turn_start(s):
        turn_copy(s).start()

    stream_copy = pltpu.make_async_copy(
        stream_grad.at[:, columns(tp, width)], stream_out, local.at[3]
    )
    with jax.named_scope("mixed_grad"):
        loop(1, n, turn_start)
        stream_copy.start()
        loads[3].wait()
        mixed_grad = jnp.dot(stream_grad[...], w_out[...], preferred_element_type=jnp.float32)
        small[0] = (mixed_grad * filtered[...]).astype(jnp.bfloat16)
        extended_grad[pl.ds(0, count), :] = mixed_grad * out_gate[...].astype(jnp.float32)

        @pl.when(me > 0)
        def _():
            halo_earlier().start()

    def turn_land(s):
        turn_copy(s).wait_recv()
        if shared_parts > 1:
            turn_part(s, tp, turn_send.at[1], turn_cross.at[s], cross).start()
            turn_part(s, tp, turn_send.at[2], turn_near.at[s], partner).start()

    def turn_forward(s):
        turn_part(s, cross, turn_send.at[1], turn_cross.at[s], cross).wait_recv()
        turn_part(s, cross, turn_send.at[3], turn_near.at[s], partner).start()

    def turn_step(s):
        turn_land(s)
        if shared_parts > 1:

            @pl.when(s > 1)
            def _():
                turn_forward(s - 1)

    with jax.named_scope("turn_land"):
        loop(1, n, turn_step)
        if shared_parts > 1:
            turn_forward(n - 1)

    with jax.named_scope("conv_grad"):
        @pl.when(me < n - 1)
        def _():
            halo_earlier().wait_recv()

        product_grad = (
            taps[0:1, :] * extended_grad[pl.ds(0, count), :]
            + taps[1:2, :] * extended_grad[pl.ds(1, count), :]
            + taps[2:3, :] * extended_grad[pl.ds(2, count), :]
        )
        small[1] = (product_grad * conv_input[...].astype(jnp.float32)).astype(jnp.bfloat16)
        small[2] = (product_grad * in_gate[...].astype(jnp.float32)).astype(jnp.bfloat16)
        small_copies = [
            pltpu.make_async_copy(small.at[i], target, local.at[4 + i])
            for i, target in enumerate((out_gate_out, in_gate_out, conv_input_out))
        ]
        for one in small_copies:
            one.start()

    w_out_sum[...] = jnp.dot(
        turned[pl.ds(pl.multiple_of(me * block, block), block), :],
        mixed[0],
        preferred_element_type=jnp.float32,
    )

    def out_step(s):
        if shared_parts > 1:
            pair_rows = turned_all.at[s, pl.ds(0, 2 * share)]
            remote(
                pair_rows, pair_rows, turn_send.at[2], turn_near.at[s], {"tp": partner}
            ).wait_recv()

        @pl.when(s < half)
        def _():
            mix_copy(0, s, s).wait_recv()

        @pl.when(s > half)
        def _():
            mix_copy(half, s, s - half).wait_recv()

        w_out_sum[...] += jnp.dot(turned_all[s], mixed[s], preferred_element_type=jnp.float32)

    with jax.named_scope("w_out_grad"):
        loop(1, n, out_step)
        last = pltpu.make_async_copy(w_out_sum, w_out_grad, local.at[7])
        last.start()

    with jax.named_scope("drain"):
        route_copy().wait_send()
        for a in (0, 1):
            token_copy(a).wait_send()
            sent = sending.at[a, pl.ds(0, (n - 2) * depth)]
            remote(sent, sent, slot_send.at[a], slot_recv.at[a, 0], {"tp": partner}).wait_send()
            most = slots.at[a, pl.ds(0, (n - 1) * depth), pl.ds(0, width)]
            for sem in (cross_send, near_send, fwd_send):
                remote(most, most, sem.at[a], near_recv.at[a, 0], {"tp": partner}).wait_send()
            remote(far_out, far_in, hand_send.at[a], hand_recv.at[a, 0], {"tp": partner}).wait_send()
        remote(far_out, far_in, far_send, far_recv.at[0], {"tp": cross}).wait_send()
        rest = total.at[pl.ds(0, (n - 1) * depth)]
        remote(rest, rest, out_send, out_recv.at[0], {"tp": partner}).wait_send()
        sent = mixed.at[pl.ds(0, n - 1)]
        remote(sent, sent, mix_send, mix_recv.at[0], {"tp": partner}).wait_send()
        sent = turned_all.at[pl.ds(0, n - 1), pl.ds(0, share)]
        for kind in range(4 if shared_parts > 1 else 1):
            remote(sent, sent, turn_send.at[kind], turn_recv.at[0], {"tp": partner}).wait_send()

        @pl.when(me < n - 1)
        def _():
            halo_later().wait_send()

        @pl.when(me > 0)
        def _():
            halo_earlier().wait_send()

        stream_copy.wait()
        for one in small_copies:
            one.wait()
        for i, (source, target) in enumerate(
            ((gate_sum, gate_out), (up_sum, up_out), (down_sum, down_out))
        ):
            pltpu.make_async_copy(source, target, local.at[i]).wait()
        last.wait()


def shards(
    cotangent,
    stream_in,
    norm_gain,
    out_gate,
    in_gate,
    conv_input,
    conv_taps,
    out_weight,
    expert_gate,
    expert_up,
    expert_down,
    expert_choice,
    route_scale,
):
    n = lax.axis_size("sp")
    count, wide = stream_in.shape
    channels = out_gate.shape[1]
    hidden = expert_gate.shape[2]
    width = wide // lax.axis_size("tp")
    depth = 4 * count // n
    rows = n * depth
    block = wide // n
    pieces = 2
    kind = stream_in.dtype
    route = jnp.concatenate(
        [expert_choice.T.astype(jnp.float32), route_scale.T, jnp.zeros((4, count), jnp.float32)]
    )

    def out(*shape, dtype=kind):
        return jax.ShapeDtypeStruct(shape, dtype)

    def full(*shape):
        return pltpu.VMEM(shape, jnp.float32)

    def held(*shape):
        return pltpu.VMEM(shape, kind)

    vmem, anywhere = (pl.BlockSpec(memory_space=pltpu.VMEM), pl.BlockSpec(memory_space=pl.ANY))
    dma = pltpu.SemaphoreType.DMA
    results = pl.pallas_call(
        functools.partial(step_kernel, n),
        out_shape=[
            out(count, width),
            out(count, channels),
            out(count, channels),
            out(count, channels),
            out(block, channels, dtype=jnp.float32),
            out(wide, hidden, dtype=jnp.float32),
            out(wide, hidden, dtype=jnp.float32),
            out(hidden, wide, dtype=jnp.float32),
        ],
        in_specs=[vmem] * 8 + [anywhere] * 4,
        out_specs=[anywhere] * 8,
        scratch_shapes=[
            held(count, wide),
            full(count, 1),
            full(count, 1),
            held(wide, channels),
            held(wide, hidden),
            held(wide, hidden),
            held(hidden, wide),
            full(2, n, count),
            full(2, n, count),
            held(2, count, width),
            full(*route.shape),
            held(2, rows, width),
            held(2, rows, wide),
            held(rows, hidden),
            held(rows, 2 * hidden),
            held(rows, wide),
            held(2, rows, width),
            held(rows, width),
            held(rows, width),
            held(rows, width),
            held(rows, width),
            full(count, width),
            held(count, wide),
            full(count + 8, channels),
            full(count, channels),
            full(count + 8, channels),
            held(n, count, channels),
            held(count, wide),
            held(wide, count),
            held(n, block, count),
            full(wide, hidden),
            full(wide, hidden),
            full(hidden, wide),
            held(3, count, channels),
            full(block, channels),
            dma((4,)),
            dma((3,)),
            dma((3,)),
            dma((2,)),
            dma((2, n)),
            dma((2,)),
            dma((2, n)),
            dma((2,)),
            dma((2,)),
            dma((2, n)),
            dma((2,)),
            dma((2, n)),
            dma,
            dma((n,)),
            dma,
            dma((n,)),
            dma((3, pieces)),
            dma((pieces,)),
            dma((2, pieces)),
            dma((2,)),
            dma((2,)),
            dma,
            dma((n,)),
            dma((4,)),
            dma((n,)),
            dma((n,)),
            dma((n,)),
            dma((8,)),
        ],
        compiler_params=pltpu.CompilerParams(
            collective_id=1, has_side_effects=True, vmem_limit_bytes=58 * 1024 * 1024
        ),
    )(
        stream_in,
        cotangent,
        norm_gain[None],
        route,
        out_gate,
        in_gate,
        conv_input,
        conv_taps,
        out_weight,
        expert_gate[0],
        expert_up[0],
        expert_down[0],
    )
    return (*results[:5], *(grad[None] for grad in results[5:]))


def solution(mesh):
    placed = (
        P("sp", None),
        P("sp", None),
        P(),
        P("sp", "tp"),
        P("sp", "tp"),
        P("sp", "tp"),
        P(None, "tp"),
        P(None, "tp"),
        P("sp", None, "tp"),
        P("sp", None, "tp"),
        P("sp", "tp", None),
        P("sp", None),
        P("sp", None),
    )
    return jax.shard_map(
        shards,
        mesh=mesh,
        in_specs=placed,
        out_specs=(
            P("sp", "tp"),
            P("sp", "tp"),
            P("sp", "tp"),
            P("sp", "tp"),
            P("sp", "tp"),
            P("sp", None, "tp"),
            P("sp", None, "tp"),
            P("sp", "tp", None),
        ),
        check_vma=False,
    )
```

time: 158 us -> 146 us (0.924)
  Pallas kernels: 102 us -> 128 us
  matrix products: 14.2 us -> 0 us
  starting transfers between devices: 14 us -> 0 us
  local copies, waits for them, and re-layouts: 1.83 us -> 15 us
  waiting for transfers between devices: 12.4 us -> 0 us
  other arithmetic: 12.6 us -> 2.03 us
    pallas_call x1, Pallas kernels: 102 us -> 128 us  [shards(): pl.pallas_call(functools.partial(step_kernel, n), out_shape=[out(count, w...]
    unnamed x24 -> x12, local copies, waits for them, and re-layouts: 0.06 us -> 14.9 us
    dot_general x5 -> x0, matrix products: 14.2 us -> none  [the longest x4 11.8 us: rows_product(): lax.dot_general(left, right, (((0,), (0,)), ((), ())), preferred_element_...]
    all_to_all x1 -> x0, waiting for transfers between devices: 9.86 us -> none  [shards(): shares = lax.all_to_all(shares, 'sp', split_axis=0, concat_axis=0)]
    all_to_all x1 -> x0, starting transfers between devices: 7.87 us -> none  [shards(): shares = lax.all_to_all(shares, 'sp', split_axis=0, concat_axis=0)]
    ppermute x2 -> x0, starting transfers between devices: 6.18 us -> none  [passed_along(): lax.ppermute(value, axis, [(source, source + steps) for source in range(f...]
    reduce_sum x3 -> x0, other arithmetic: 5.53 us -> none  [the longest x1 2.09 us: shards(): grad_out_weight = jnp.sum(shares.astype(jnp.float32), axis=0)]
    convert_element_type x4 -> x0, other arithmetic: 5.15 us -> none  [the longest x1 1.97 us: shards(): normed = (unit_stream * norm_gain).astype(jnp.bfloat16)]
  transfers between devices with their start and end apart: 3 -> 0, of which waited for: 2 -> 0; matrix products, arithmetic and copies ran while one was open for 14% -> 0% of each run, Pallas kernels for 65% -> 0%
where the time goes in v2:
time: 146 us
  Pallas kernels  128 us (88%)
  local copies, waits for them, and re-layouts  15 us (10%)
  other arithmetic  2.03 us (1%)
    pallas_call x1, Pallas kernels, shards(): pl.pallas_call(functools.partial(step_kernel, n), out_shape=[out(count, w...  128 us
    unnamed x12, local copies, waits for them, and re-layouts  14.9 us

profile of v2, /device:TPU:0, one launch (start us, length us, event | category | flops | bytes accessed | tf_op | source)
XLA Modules:
  0.0 145.9 jit_solution(12131332822396807172)
XLA Ops:
  0.6 0.1 pad.2.clone
  0.7 0.7 convert_bitcast_fusion
  1.4 1.3 maximum_maximum_fusion.route
  2.8 128.2 %shard_map.188 = (bf16[256,512]{1,0:T(8,128)(2,1)}, bf16[256,256]{1,0:T(8,128)(2,1)}, bf16[256,256]{1,0:T(8,128)(2,1)}, bf16[256,256]{1,0:T(8,128)(2,1)}, f32[25...) custom-call(bf16[256,2048]{1,0:T(8,128)(2,1)} %stream.1, ...), custom_call_target="tpu_custom_call" | custom-call | tf_op jit(solution)/shard_map/pallas_call | solution.py:769
  131.0 1.7 %copy.29 = bf16[256,512]{1,0:T(8,128)(2,1)} copy(bf16[256,512]{1,0:T(8,128)(2,1)} %get-tuple-element.32) | data formatting | bytes 524288
  132.6 1.6 %copy.30 = bf16[256,256]{1,0:T(8,128)(2,1)} copy(bf16[256,256]{1,0:T(8,128)(2,1)} %get-tuple-element.33) | data formatting | bytes 262144
  134.2 1.6 %copy.31 = bf16[256,256]{1,0:T(8,128)(2,1)} copy(bf16[256,256]{1,0:T(8,128)(2,1)} %get-tuple-element.34) | data formatting | bytes 262144
  135.8 1.6 %copy.32 = bf16[256,256]{1,0:T(8,128)(2,1)} copy(bf16[256,256]{1,0:T(8,128)(2,1)} %get-tuple-element.35) | data formatting | bytes 262144
  137.3 1.7 %copy.33 = f32[256,256]{1,0:T(8,128)} copy(f32[256,256]{1,0:T(8,128)} %get-tuple-element.36) | data formatting | bytes 524288
  139.0 0.0 copy-start.1
  139.0 3.2 %copy.34 = f32[1,2048,256]{2,1,0:T(8,128)} copy(f32[1,2048,256]{2,1,0:T(8,128)} %bitcast.12) | data formatting | bytes 4194304
  142.2 0.0 copy-done.1
  142.2 0.0 copy-start
  142.2 1.3 copy.35
  143.5 1.0 copy-done
  144.6 1.3 copy.36
  (1 shorter events, 0.0 us)
Async XLA Ops:
  139.0 3.2 %copy-start.1 = (f32[2048,256]{1,0:T(8,128)S(1)}, f32[2048,256]{1,0:T(8,128)}, u32[]{:S(2)}) copy-start(f32[2048,256]{1,0:T(8,128)} %get-tuple-element.22) | copy-start | bytes 6291460
  142.2 2.3 %copy-start = (f32[256,2048]{1,0:T(8,128)S(1)}, f32[256,2048]{1,0:T(8,128)}, u32[]{:S(2)}) copy-start(f32[256,2048]{1,0:T(8,128)} %get-tuple-element.23) | copy-start | bytes 6291460

commit v3 on v2

--- a/solution.py
+++ b/solution.py
@@ -8,6 +8,7 @@
 from jax.sharding import PartitionSpec as P
 
 norm_eps = 1e-06
+VMEM = 39 * 1024 * 1024
 
 
 def rows_product(left, right):
@@ -83,7 +84,8 @@
     stream,
     cot,
     gain,
-    route,
+    choice,
+    scales,
     out_gate,
     in_gate,
     conv_input,
@@ -93,13 +95,11 @@
     w_up_hbm,
     w_down_hbm,
     stream_out,
-    out_gate_out,
-    in_gate_out,
-    conv_input_out,
-    w_out_grad,
-    gate_out,
-    up_out,
-    down_out,
+    small_out,
+    w_out_sum,
+    gate_sum,
+    up_sum,
+    down_sum,
     normed,
     inverse,
     along,
@@ -110,7 +110,8 @@
     keys,
     weights,
     arrived,
-    arrived_route,
+    arrived_choice,
+    arrived_scales,
     sending,
     slots,
     hidden,
@@ -130,11 +131,6 @@
     stream_grad,
     turned,
     turned_all,
-    gate_sum,
-    up_sum,
-    down_sum,
-    small,
-    w_out_sum,
     load,
     tok_send,
     tok_recv,
@@ -162,7 +158,6 @@
     turn_recv,
     turn_cross,
     turn_near,
-    local,
 ):
     me = lax.axis_index("sp")
     tp, cross, partner, diagonal = tp_places()
@@ -202,9 +197,10 @@
         inverse[rows, :] = scale
         normed[rows, :] = (values * scale * gain[...]).astype(jnp.bfloat16)
 
-    def table(which, source):
-        c0, c1, s0, s1 = (source[i : i + 1, :] for i in range(4))
-        expert = lax.broadcasted_iota(jnp.int32, (n, count), 0).astype(jnp.float32)
+    def table(which, named, scaled):
+        c0, c1 = (named[i : i + 1, :] for i in range(2))
+        s0, s1 = (scaled[i : i + 1, :] for i in range(2))
+        expert = lax.broadcasted_iota(jnp.int32, (n, count), 0)
         first, second = (c0 == expert, c1 == expert)
         member = jnp.where(first | second, 1.0, 0.0)
         row = lax.broadcasted_iota(jnp.int32, (count, count), 0)
@@ -241,8 +237,12 @@
             {"sp": other(half)},
         )
 
-    def route_copy():
-        return remote(route, arrived_route, tok_send.at[2], tok_recv.at[2], {"sp": other(half)})
+    def route_copies():
+        pairs = ((choice, arrived_choice), (scales, arrived_scales))
+        return [
+            remote(source, target, tok_send.at[2 + i], tok_recv.at[2 + i], {"sp": other(half)})
+            for i, (source, target) in enumerate(pairs)
+        ]
 
     def slot_copy(a, s, k):
         return remote(
@@ -314,7 +314,7 @@
 
     with jax.named_scope("prep"):
         loop(0, count // 32, normalize)
-        table(0, route)
+        table(0, choice, scales)
         product = in_gate[...].astype(jnp.float32) * conv_input[...].astype(jnp.float32)
         extended[pl.ds(8, count), :] = product
 
@@ -337,8 +337,9 @@
 
     with jax.named_scope("send_own"):
         loop(1, half, send_own)
+        for one in route_copies():
+            one.start()
         token_copy(0).start()
-        route_copy().start()
         token_copy(1).start()
 
         @pl.when(me < n - 1)
@@ -377,8 +378,9 @@
     for a in (0, 1):
         with jax.named_scope("await_tokens"):
             if a == 0:
-                route_copy().wait_recv()
-                table(1, arrived_route)
+                for one in route_copies():
+                    one.wait_recv()
+                table(1, arrived_choice, arrived_scales)
             token_copy(a).wait_recv()
 
         def send_other(k):
@@ -452,37 +454,42 @@
     def land_other(k):
         land(half + k, k)
 
-        @pl.when(k == 1)
-        def _():
-            forward_both(half)
-
-        @pl.when(k > 1)
-        def _():
-            forward_both(half + k - 1)
-
-    with jax.named_scope("land_other"):
-        loop(1, half, land_other)
-
     def pair(s):
         hand(1, s).wait_recv()
         mine = partial[at(s), columns(cross, width)].astype(jnp.float32)
         far_out[at(s), :] = (mine + near[1, at(s), :].astype(jnp.float32)).astype(jnp.bfloat16)
         across(s).start()
 
+    with jax.named_scope("land_other"):
+        loop(1, half, land_other)
+        mix_copy(half, half, half).wait_recv()
+
+        def mix_other(k):
+            mix_copy(half, half + k, k).start()
+
+        loop(1, half, mix_other)
+
+    def forward_group(g):
+        loop(0, group, lambda i: forward_both(g * group + i))
+
+    def pair_group(g):
+        loop(0, group, lambda i: pair(g * group + i))
+
+    def work_other(g):
+        with jax.named_scope("forward_group"):
+            forward_group(g)
+        with jax.named_scope("work_group"):
+            work(g)
+
+        @pl.when(g < groups - 1)
+        def _():
+            pair_group(g)
+
+    loop(groups // 2, groups, work_other)
     with jax.named_scope("pair_own"):
         loop(0, half, pair)
-        mix_copy(half, half, half).wait_recv()
-
-        def mix_other(k):
-            mix_copy(half, half + k, k).start()
-
-        loop(1, half, mix_other)
-    with jax.named_scope("forward_last"):
-        forward_both(n - 1)
-    with jax.named_scope("work_other"):
-        loop(groups // 2, groups, work)
-    with jax.named_scope("pair_other"):
-        loop(half, n, pair)
+    with jax.named_scope("pair_last"):
+        pair_group(groups - 1)
 
     def finish(s):
         hand(0, s).wait_recv()
@@ -496,37 +503,25 @@
         total[at(s), :] = finish(s)
         give(s).start()
 
-    def grad_copies(c):
-        rows = pl.ds(pl.multiple_of(c * chunk, chunk), chunk)
-        return [
-            pltpu.make_async_copy(source, target, local.at[i])
-            for i, (source, target) in enumerate(
-                (
-                    (gate_sum.at[rows, :], gate_out.at[rows, :]),
-                    (up_sum.at[rows, :], up_out.at[rows, :]),
-                    (down_sum.at[:, rows], down_out.at[:, rows]),
-                )
-            )
-        ]
-
     def grads(c):
         rows = pl.ds(pl.multiple_of(c * chunk, chunk), chunk)
         sums = rows_product(slots[0, :, rows], both_grad[...])
         gate_sum[rows, :] = sums[:, : sums.shape[1] // 2]
         up_sum[rows, :] = sums[:, sums.shape[1] // 2 :]
         down_sum[:, rows] = rows_product(hidden[...], slots[1, :, rows])
-        for one in grad_copies(c):
-            one.start()
-
+
+    pieces_of = wide // chunk
+    with jax.named_scope("finish_other"):
+        loop(half, n - group, finish_one)
+    with jax.named_scope("grads"):
+        loop(0, pieces_of // 2, grads)
     with jax.named_scope("finish_own"):
         loop(1, half, finish_one)
         back[pl.ds(0, depth), :] = finish(0)
+    with jax.named_scope("finish_last"):
+        loop(n - group, n, finish_one)
     with jax.named_scope("grads"):
-        loop(0, wide // chunk // 2, grads)
-    with jax.named_scope("finish_other"):
-        loop(half, n, finish_one)
-    with jax.named_scope("grads"):
-        loop(wide // chunk // 2, wide // chunk, grads)
+        loop(pieces_of // 2, pieces_of, grads)
     acc[...] = jnp.zeros_like(acc)
 
     def combine(s):
@@ -604,15 +599,12 @@
     def turn_start(s):
         turn_copy(s).start()
 
-    stream_copy = pltpu.make_async_copy(
-        stream_grad.at[:, columns(tp, width)], stream_out, local.at[3]
-    )
     with jax.named_scope("mixed_grad"):
         loop(1, n, turn_start)
-        stream_copy.start()
+        stream_out[...] = stream_grad[:, columns(tp, width)]
         loads[3].wait()
         mixed_grad = jnp.dot(stream_grad[...], w_out[...], preferred_element_type=jnp.float32)
-        small[0] = (mixed_grad * filtered[...]).astype(jnp.bfloat16)
+        small_out[0] = (mixed_grad * filtered[...]).astype(jnp.bfloat16)
         extended_grad[pl.ds(0, count), :] = mixed_grad * out_gate[...].astype(jnp.float32)
 
         @pl.when(me > 0)
@@ -629,18 +621,11 @@
         turn_part(s, cross, turn_send.at[1], turn_cross.at[s], cross).wait_recv()
         turn_part(s, cross, turn_send.at[3], turn_near.at[s], partner).start()
 
-    def turn_step(s):
-        turn_land(s)
+    with jax.named_scope("turn_land"):
+        loop(1, n, turn_land)
+    with jax.named_scope("turn_forward"):
         if shared_parts > 1:
-
-            @pl.when(s > 1)
-            def _():
-                turn_forward(s - 1)
-
-    with jax.named_scope("turn_land"):
-        loop(1, n, turn_step)
-        if shared_parts > 1:
-            turn_forward(n - 1)
+            loop(1, n, turn_forward)
 
     with jax.named_scope("conv_grad"):
         @pl.when(me < n - 1)
@@ -652,14 +637,8 @@
             + taps[1:2, :] * extended_grad[pl.ds(1, count), :]
             + taps[2:3, :] * extended_grad[pl.ds(2, count), :]
         )
-        small[1] = (product_grad * conv_input[...].astype(jnp.float32)).astype(jnp.bfloat16)
-        small[2] = (product_grad * in_gate[...].astype(jnp.float32)).astype(jnp.bfloat16)
-        small_copies = [
-            pltpu.make_async_copy(small.at[i], target, local.at[4 + i])
-            for i, target in enumerate((out_gate_out, in_gate_out, conv_input_out))
-        ]
-        for one in small_copies:
-            one.start()
+        small_out[1] = (product_grad * conv_input[...].astype(jnp.float32)).astype(jnp.bfloat16)
+        small_out[2] = (product_grad * in_gate[...].astype(jnp.float32)).astype(jnp.bfloat16)
 
     w_out_sum[...] = jnp.dot(
         turned[pl.ds(pl.multiple_of(me * block, block), block), :],
@@ -686,11 +665,10 @@
 
     with jax.named_scope("w_out_grad"):
         loop(1, n, out_step)
-        last = pltpu.make_async_copy(w_out_sum, w_out_grad, local.at[7])
-        last.start()
 
     with jax.named_scope("drain"):
-        route_copy().wait_send()
+        for one in route_copies():
+            one.wait_send()
         for a in (0, 1):
             token_copy(a).wait_send()
             sent = sending.at[a, pl.ds(0, (n - 2) * depth)]
@@ -716,14 +694,18 @@
         def _():
             halo_earlier().wait_send()
 
-        stream_copy.wait()
-        for one in small_copies:
-            one.wait()
-        for i, (source, target) in enumerate(
-            ((gate_sum, gate_out), (up_sum, up_out), (down_sum, down_out))
-        ):
-            pltpu.make_async_copy(source, target, local.at[i]).wait()
-        last.wait()
+
+def store_kernel(stream, small, w_out, gate, up, down, *rest):
+    outs, local = rest[:8], rest[8]
+    ins = (stream, small.at[0], small.at[1], small.at[2], w_out, gate, up, down)
+    copies = [
+        pltpu.make_async_copy(source, target, local.at[i])
+        for i, (source, target) in enumerate(zip(ins, outs))
+    ]
+    for one in copies:
+        one.start()
+    for one in copies:
+        one.wait()
 
 
 def shards(
@@ -751,9 +733,6 @@
     block = wide // n
     pieces = 2
     kind = stream_in.dtype
-    route = jnp.concatenate(
-        [expert_choice.T.astype(jnp.float32), route_scale.T, jnp.zeros((4, count), jnp.float32)]
-    )
 
     def out(*shape, dtype=kind):
         return jax.ShapeDtypeStruct(shape, dtype)
@@ -770,16 +749,14 @@
         functools.partial(step_kernel, n),
         out_shape=[
             out(count, width),
-            out(count, channels),
-            out(count, channels),
-            out(count, channels),
+            out(3, count, channels),
             out(block, channels, dtype=jnp.float32),
             out(wide, hidden, dtype=jnp.float32),
             out(wide, hidden, dtype=jnp.float32),
             out(hidden, wide, dtype=jnp.float32),
         ],
-        in_specs=[vmem] * 8 + [anywhere] * 4,
-        out_specs=[anywhere] * 8,
+        in_specs=[vmem] * 9 + [anywhere] * 4,
+        out_specs=[vmem] * 6,
         scratch_shapes=[
             held(count, wide),
             full(count, 1),
@@ -791,7 +768,8 @@
             full(2, n, count),
             full(2, n, count),
             held(2, count, width),
-            full(*route.shape),
+            pltpu.VMEM((2, count), jnp.int32),
+            full(2, count),
             held(2, rows, width),
             held(2, rows, wide),
             held(rows, hidden),
@@ -811,14 +789,9 @@
             held(count, wide),
             held(wide, count),
             held(n, block, count),
-            full(wide, hidden),
-            full(wide, hidden),
-            full(hidden, wide),
-            held(3, count, channels),
-            full(block, channels),
             dma((4,)),
-            dma((3,)),
-            dma((3,)),
+            dma((4,)),
+            dma((4,)),
             dma((2,)),
             dma((2, n)),
             dma((2,)),
@@ -843,26 +816,43 @@
             dma((n,)),
             dma((n,)),
             dma((n,)),
-            dma((8,)),
         ],
         compiler_params=pltpu.CompilerParams(
-            collective_id=1, has_side_effects=True, vmem_limit_bytes=58 * 1024 * 1024
+            collective_id=1, has_side_effects=True, vmem_limit_bytes=VMEM + 2 * n * count * channels
         ),
     )(
         stream_in,
         cotangent,
         norm_gain[None],
-        route,
+        expert_choice.T,
+        route_scale.T,
         out_gate,
         in_gate,
         conv_input,
         conv_taps,
-        out_weight,
-        expert_gate[0],
-        expert_up[0],
-        expert_down[0],
+        *(
+            pltpu.with_memory_space_constraint(weight, pltpu.HBM)
+            for weight in (out_weight, expert_gate[0], expert_up[0], expert_down[0])
+        ),
     )
-    return (*results[:5], *(grad[None] for grad in results[5:]))
+    stored = pl.pallas_call(
+        store_kernel,
+        out_shape=[
+            out(count, width),
+            out(count, channels),
+            out(count, channels),
+            out(count, channels),
+            out(block, channels, dtype=jnp.float32),
+            out(wide, hidden, dtype=jnp.float32),
+            out(wide, hidden, dtype=jnp.float32),
+            out(hidden, wide, dtype=jnp.float32),
+        ],
+        in_specs=[vmem] * 6,
+        out_specs=[anywhere] * 8,
+        scratch_shapes=[dma((8,))],
+        compiler_params=pltpu.CompilerParams(vmem_limit_bytes=9 * 1024 * 1024),
+    )(*results)
+    return (*stored[:5], *(grad[None] for grad in stored[5:]))
 
 
 def solution(mesh):

time: 146 us -> 129 us (0.88)
  Pallas kernels: 128 us -> 120 us
  local copies, waits for them, and re-layouts: 15 us -> 7.9 us
  other arithmetic: 2.03 us -> 0 us
    pallas_call x1, Pallas kernels: 128 us -> 117 us  [shards(): pl.pallas_call(functools.partial(step_kernel, n), out_shape=[out(count, w...]
    unnamed x12 -> x18, local copies, waits for them, and re-layouts: 14.9 us -> 7.9 us
    pallas_call x0 -> x1, Pallas kernels: none -> 3.07 us  [shards(): pl.pallas_call(store_kernel, out_shape=[out(count, width), out(count, cha...]
where the time goes in v3:
time: 129 us; the launch traced here: 128 us
  Pallas kernels  120 us (93%)
  local copies, waits for them, and re-layouts  7.9 us (6%)
    pallas_call x1, Pallas kernels, shards(): pl.pallas_call(functools.partial(step_kernel, n), out_shape=[out(count, w...  117 us
    unnamed x18, local copies, waits for them, and re-layouts  7.9 us
    pallas_call x1, Pallas kernels, shards(): pl.pallas_call(store_kernel, out_shape=[out(count, width), out(count, cha...  3.07 us

profile of v3, /device:TPU:0, one launch (start us, length us, event | category | flops | bytes accessed | tf_op | source)
XLA Modules:
  0.0 128.3 jit_solution(2449123134153566507)
XLA Ops:
  0.6 0.0 copy-start
  0.6 1.2 copy-done
  1.9 0.0 copy-start.1
  1.9 1.2 copy-done.1
  3.1 0.0 copy-start.2
  3.1 0.9 copy-done.2
  4.0 0.0 copy-start.3
  4.0 0.9 copy-done.3
  4.9 0.0 copy-start.4
  4.9 0.9 copy-done.4
  5.8 0.0 copy-start.5
  5.8 0.7 copy-done.5
  6.5 0.0 copy-start.6
  6.5 0.7 copy-done.6
  7.2 0.0 copy-start.7
  7.2 0.7 copy-done.7
  7.9 0.0 copy-start.8
  7.9 0.7 copy-done.8
  8.6 116.7 %shard_map.188 = (bf16[256,512]{1,0:T(8,128)(2,1)S(1)}, bf16[3,256,256]{2,1,0:T(8,128)(2,1)S(1)}, f32[256,256]{1,0:T(8,128)S(1)}, f32[2048,256]{1,0:T(8,128)S(1)...) custom-call(bf16[256,2048]{1,0:T(8,128)(2,1)S(1)} %copy-done, bf16[256,2048]{1,0:T(8,128)(2,1)S(1)} %copy-done.1, ...), custom_call_target="tpu_custom_call" | custom-call | tf_op jit(solution)/shard_map/pallas_call | solution.py:748
  125.2 3.1 %shard_map.189 = (bf16[256,512]{1,0:T(8,128)(2,1)}, bf16[256,256]{1,0:T(8,128)(2,1)}, bf16[256,256]{1,0:T(8,128)(2,1)}, bf16[256,256]{1,0:T(8,128)(2,1)}, f32[25...) custom-call(bf16[256,512]{1,0:T(8,128)(2,1)S(1)} %get-tuple-element.22.stream, ...), custom_call_target="tpu_custom_call" | custom-call | tf_op jit(solution)/shard_map/pallas_call | solution.py:838
Async XLA Ops:
  0.6 1.2 copy-start
  1.9 1.2 copy-start.1
  3.1 0.9 copy-start.2
  4.0 0.9 copy-start.3
  4.9 0.9 copy-start.4
  5.8 0.7 copy-start.5
  6.5 0.7 copy-start.6
  7.2 0.7 copy-start.7
  7.9 0.7 copy-start.8

commit v4 on v3

--- a/solution.py
+++ b/solution.py
@@ -8,7 +8,7 @@
 from jax.sharding import PartitionSpec as P
 
 norm_eps = 1e-06
-VMEM = 39 * 1024 * 1024
+VMEM = 42 * 1024 * 1024
 
 
 def rows_product(left, right):
@@ -81,91 +81,94 @@
 
 def step_kernel(
     n,
-    stream,
-    cot,
-    gain,
-    choice,
-    scales,
-    out_gate,
-    in_gate,
-    conv_input,
-    taps,
-    w_out_hbm,
-    w_gate_hbm,
-    w_up_hbm,
-    w_down_hbm,
-    stream_out,
-    small_out,
-    w_out_sum,
-    gate_sum,
-    up_sum,
-    down_sum,
-    normed,
-    inverse,
-    along,
-    w_out,
-    w_gate,
-    w_up,
-    w_down,
-    keys,
-    weights,
-    arrived,
-    arrived_choice,
-    arrived_scales,
-    sending,
-    slots,
-    hidden,
-    both_grad,
-    partial,
-    near,
-    far_out,
-    far_in,
-    total,
-    back,
-    acc,
-    token,
-    extended,
-    filtered,
-    extended_grad,
-    mixed,
-    stream_grad,
-    turned,
-    turned_all,
-    load,
-    tok_send,
-    tok_recv,
-    slot_send,
-    slot_recv,
-    cross_send,
-    cross_recv,
-    near_send,
-    fwd_send,
-    near_recv,
-    hand_send,
-    hand_recv,
-    far_send,
-    far_recv,
-    out_send,
-    out_recv,
-    all_send,
-    all_cross,
-    all_near,
-    halo_send,
-    halo_recv,
-    mix_send,
-    mix_recv,
-    turn_send,
-    turn_recv,
-    turn_cross,
-    turn_near,
+    *refs,
 ):
+    inputs, refs = refs[:13], refs[13:]
+    (
+        stream_out,
+        small_out,
+        w_out_sum,
+        gate_sum,
+        up_sum,
+        down_sum,
+        normed,
+        inverse,
+        along,
+        keys,
+        weights,
+        arrived,
+        arrived_choice,
+        arrived_scales,
+        sending,
+        slots,
+        hidden,
+        both_grad,
+        partial,
+        near,
+        far_out,
+        far_in,
+        total,
+        back,
+        acc,
+        token,
+        extended,
+        filtered,
+        extended_grad,
+        mixed,
+        stream_grad,
+        turned,
+        turned_all,
+        load,
+        tok_send,
+        tok_recv,
+        slot_send,
+        slot_recv,
+        cross_send,
+        cross_recv,
+        near_send,
+        fwd_send,
+        near_recv,
+        hand_send,
+        hand_recv,
+        far_send,
+        far_recv,
+        out_send,
+        out_recv,
+        all_send,
+        all_cross,
+        all_near,
+        halo_send,
+        halo_recv,
+        mix_send,
+        mix_recv,
+        turn_send,
+        turn_recv,
+        turn_cross,
+        turn_near,
+    ) = refs[:6] + refs[19:]
+    loaded = refs[6:19]
+    (
+        stream,
+        cot,
+        gain,
+        choice,
+        scales,
+        out_gate,
+        in_gate,
+        conv_input,
+        taps,
+        w_out,
+        w_gate,
+        w_up,
+        w_down,
+    ) = loaded
     me = lax.axis_index("sp")
     tp, cross, partner, diagonal = tp_places()
     half = n // 2
     count, wide = normed.shape
     width = acc.shape[1]
     depth = near.shape[1] // n
-    group = max(1, 256 // depth)
+    group = max(1, n // 4)
     span = group * depth
     chunk = min(256, width)
     channels = filtered.shape[1]
@@ -175,11 +178,11 @@
     share = block // shared_parts
     wait_all = greet(cross, partner)
     sources = (normed, cot)
+    edge = lax.rem(lax.div(me, max(1, n // 4)) + 1, 4) < 2
+    inner = jnp.logical_not(edge)
     loads = [
         pltpu.make_async_copy(source, target, load.at[i])
-        for i, (source, target) in enumerate(
-            ((w_gate_hbm, w_gate), (w_up_hbm, w_up), (w_down_hbm, w_down), (w_out_hbm, w_out))
-        )
+        for i, (source, target) in enumerate(zip(inputs, loaded))
     ]
     for one in loads:
         one.start()
@@ -313,8 +316,14 @@
         )
 
     with jax.named_scope("prep"):
+        loads[0].wait()
+        loads[2].wait()
         loop(0, count // 32, normalize)
+        loads[3].wait()
+        loads[4].wait()
         table(0, choice, scales)
+        loads[6].wait()
+        loads[7].wait()
         product = in_gate[...].astype(jnp.float32) * conv_input[...].astype(jnp.float32)
         extended[pl.ds(8, count), :] = product
 
@@ -328,6 +337,7 @@
 
     with jax.named_scope("barrier"):
         wait_all()
+        loads[1].wait()
 
     def send_own(k):
         for a in (0, 1):
@@ -336,11 +346,16 @@
             slot_copy(a, k, k).start()
 
     with jax.named_scope("send_own"):
-        loop(1, half, send_own)
-        for one in route_copies():
-            one.start()
-        token_copy(0).start()
-        token_copy(1).start()
+        loop(1, group, send_own)
+
+        @pl.when(edge)
+        def _():
+            for one in route_copies():
+                one.start()
+            token_copy(0).start()
+            token_copy(1).start()
+
+        loop(group, half, send_own)
 
         @pl.when(me < n - 1)
         def _():
@@ -360,34 +375,28 @@
     def land_own(k):
         land(k, k)
 
-    with jax.named_scope("land_own"):
-        loop(1, half, land_own)
-
-    with jax.named_scope("filter"):
-        @pl.when(me > 0)
-        def _():
-            halo_later().wait_recv()
-
-        filtered[...] = (
-            taps[0:1, :] * extended[pl.ds(8, count), :]
-            + taps[1:2, :] * extended[pl.ds(7, count), :]
-            + taps[2:3, :] * extended[pl.ds(6, count), :]
-        )
-        mixed[0] = (out_gate[...].astype(jnp.float32) * filtered[...]).astype(jnp.bfloat16)
-
-    for a in (0, 1):
-        with jax.named_scope("await_tokens"):
+    def land_other(k):
+        land(half + k, k)
+
+    def take_tokens():
+        for a in (0, 1):
             if a == 0:
                 for one in route_copies():
                     one.wait_recv()
                 table(1, arrived_choice, arrived_scales)
             token_copy(a).wait_recv()
 
-        def send_other(k):
-            sending[a, at(half + k), :] = chosen(a, 1, other(k), arrived[a])
-            slot_copy(a, half + k, k).start()
-
-        with jax.named_scope("send_other"):
+            @pl.when(inner)
+            def _():
+                if a == 0:
+                    for one in route_copies():
+                        one.start()
+                token_copy(a).start()
+
+            def send_other(k):
+                sending[a, at(half + k), :] = chosen(a, 1, other(k), arrived[a])
+                slot_copy(a, half + k, k).start()
+
             loop(1, half, send_other)
             slots[a, at(half), columns(tp, width)] = chosen(a, 1, me, arrived[a])
             spread(a, half)
@@ -396,14 +405,13 @@
         for a in (0, 1):
             forward(a, s)
 
-    with jax.named_scope("forward_own"):
+    def mix_early():
         mix_copy(0, half, half).start()
-
-        def mix_own(k):
-            mix_copy(0, k, k).start()
-
-        loop(1, half, mix_own)
-        loop(1, half, forward_both)
+        loop(1, half, lambda k: mix_copy(0, k, k).start())
+
+    def mix_late():
+        mix_copy(half, half, half).wait_recv()
+        loop(1, half, lambda k: mix_copy(half, half + k, k).start())
 
     def compute(g):
         rows = pl.ds(pl.multiple_of(g * span, span), span)
@@ -445,51 +453,27 @@
 
         loop(0, group, hand_one)
 
-    groups = n // group
-    with jax.named_scope("work_own"):
-        for i in range(3):
-            loads[i].wait()
-        loop(0, groups // 2, work)
-
-    def land_other(k):
-        land(half + k, k)
-
     def pair(s):
         hand(1, s).wait_recv()
         mine = partial[at(s), columns(cross, width)].astype(jnp.float32)
         far_out[at(s), :] = (mine + near[1, at(s), :].astype(jnp.float32)).astype(jnp.bfloat16)
         across(s).start()
 
-    with jax.named_scope("land_other"):
-        loop(1, half, land_other)
-        mix_copy(half, half, half).wait_recv()
-
-        def mix_other(k):
-            mix_copy(half, half + k, k).start()
-
-        loop(1, half, mix_other)
-
-    def forward_group(g):
-        loop(0, group, lambda i: forward_both(g * group + i))
-
     def pair_group(g):
         loop(0, group, lambda i: pair(g * group + i))
 
-    def work_other(g):
+    def step(g):
+        def forward_one(i):
+            s = g * group + i
+
+            @pl.when(s > 0)
+            def _():
+                forward_both(s)
+
         with jax.named_scope("forward_group"):
-            forward_group(g)
+            loop(0, group, forward_one)
         with jax.named_scope("work_group"):
             work(g)
-
-        @pl.when(g < groups - 1)
-        def _():
-            pair_group(g)
-
-    loop(groups // 2, groups, work_other)
-    with jax.named_scope("pair_own"):
-        loop(0, half, pair)
-    with jax.named_scope("pair_last"):
-        pair_group(groups - 1)
 
     def finish(s):
         hand(0, s).wait_recv()
@@ -510,16 +494,94 @@
         up_sum[rows, :] = sums[:, sums.shape[1] // 2 :]
         down_sum[:, rows] = rows_product(hidden[...], slots[1, :, rows])
 
+    def finish_group(g):
+        def one(i):
+            s = g * group + i
+
+            @pl.when(s > 0)
+            def _():
+                finish_one(s)
+
+            @pl.when(s == 0)
+            def _():
+                back[pl.ds(0, depth), :] = finish(0)
+
+        loop(0, group, one)
+
+    with jax.named_scope("land_near"):
+        loop(1, group, land_own)
+    with jax.named_scope("filter"):
+        @pl.when(me > 0)
+        def _():
+            halo_later().wait_recv()
+
+        loads[5].wait()
+        loads[8].wait()
+        filtered[...] = (
+            taps[0:1, :] * extended[pl.ds(8, count), :]
+            + taps[1:2, :] * extended[pl.ds(7, count), :]
+            + taps[2:3, :] * extended[pl.ds(6, count), :]
+        )
+        mixed[0] = (out_gate[...].astype(jnp.float32) * filtered[...]).astype(jnp.bfloat16)
+
+    with jax.named_scope("land_first"):
+
+        @pl.when(inner)
+        def _():
+            take_tokens()
+            loop(1, group, land_other)
+            loop(group, half, land_own)
+
+        @pl.when(edge)
+        def _():
+            loop(group, half, land_own)
+
+    for i in range(10, 13):
+        loads[i].wait()
+    step(jnp.where(edge, 0, 2))
+    with jax.named_scope("land_second"):
+
+        @pl.when(inner)
+        def _():
+            pair_group(2)
+            loop(group, half, land_other)
+
+        @pl.when(edge)
+        def _():
+            take_tokens()
+            loop(1, half, land_other)
+
+    mix_early()
+    step(jnp.where(edge, 1, 0))
+    step(jnp.where(edge, 2, 1))
+    with jax.named_scope("return_far"):
+
+        @pl.when(inner)
+        def _():
+            finish_group(2)
+
+        @pl.when(edge)
+        def _():
+            pair_group(2)
+
+        mix_late()
+    step(3)
     pieces_of = wide // chunk
-    with jax.named_scope("finish_other"):
-        loop(half, n - group, finish_one)
+    with jax.named_scope("pairs"):
+        pair_group(0)
+        pair_group(3)
+        pair_group(1)
+
+        @pl.when(edge)
+        def _():
+            finish_group(2)
+
     with jax.named_scope("grads"):
         loop(0, pieces_of // 2, grads)
-    with jax.named_scope("finish_own"):
-        loop(1, half, finish_one)
-        back[pl.ds(0, depth), :] = finish(0)
-    with jax.named_scope("finish_last"):
-        loop(n - group, n, finish_one)
+    with jax.named_scope("finish"):
+        finish_group(0)
+        finish_group(3)
+        finish_group(1)
     with jax.named_scope("grads"):
         loop(pieces_of // 2, pieces_of, grads)
     acc[...] = jnp.zeros_like(acc)
@@ -596,13 +658,13 @@
         rows = turned_all.at[s, part_rows(part)]
         return remote(rows, rows, send, recv, {"tp": peer})
 
-    def turn_start(s):
-        turn_copy(s).start()
+    def turn_start(k):
+        turn_copy(n - k).start()
 
     with jax.named_scope("mixed_grad"):
         loop(1, n, turn_start)
         stream_out[...] = stream_grad[:, columns(tp, width)]
-        loads[3].wait()
+        loads[9].wait()
         mixed_grad = jnp.dot(stream_grad[...], w_out[...], preferred_element_type=jnp.float32)
         small_out[0] = (mixed_grad * filtered[...]).astype(jnp.bfloat16)
         extended_grad[pl.ds(0, count), :] = mixed_grad * out_gate[...].astype(jnp.float32)
@@ -745,6 +807,21 @@
 
     vmem, anywhere = (pl.BlockSpec(memory_space=pltpu.VMEM), pl.BlockSpec(memory_space=pl.ANY))
     dma = pltpu.SemaphoreType.DMA
+    operands = (
+        stream_in,
+        cotangent,
+        norm_gain[None],
+        expert_choice.T,
+        route_scale.T,
+        out_gate,
+        in_gate,
+        conv_input,
+        conv_taps,
+        out_weight,
+        expert_gate[0],
+        expert_up[0],
+        expert_down[0],
+    )
     results = pl.pallas_call(
         functools.partial(step_kernel, n),
         out_shape=[
@@ -755,16 +832,13 @@
             out(wide, hidden, dtype=jnp.float32),
             out(hidden, wide, dtype=jnp.float32),
         ],
-        in_specs=[vmem] * 9 + [anywhere] * 4,
+        in_specs=[anywhere] * 13,
         out_specs=[vmem] * 6,
-        scratch_shapes=[
+        scratch_shapes=[pltpu.VMEM(x.shape, x.dtype) for x in operands]
+        + [
             held(count, wide),
             full(count, 1),
             full(count, 1),
-            held(wide, channels),
-            held(wide, hidden),
-            held(wide, hidden),
-            held(hidden, wide),
             full(2, n, count),
             full(2, n, count),
             held(2, count, width),
@@ -789,7 +863,7 @@
             held(count, wide),
             held(wide, count),
             held(n, block, count),
-            dma((4,)),
+            dma((13,)),
             dma((4,)),
             dma((4,)),
             dma((2,)),
@@ -820,21 +894,7 @@
         compiler_params=pltpu.CompilerParams(
             collective_id=1, has_side_effects=True, vmem_limit_bytes=VMEM + 2 * n * count * channels
         ),
-    )(
-        stream_in,
-        cotangent,
-        norm_gain[None],
-        expert_choice.T,
-        route_scale.T,
-        out_gate,
-        in_gate,
-        conv_input,
-        conv_taps,
-        *(
-            pltpu.with_memory_space_constraint(weight, pltpu.HBM)
-            for weight in (out_weight, expert_gate[0], expert_up[0], expert_down[0])
-        ),
-    )
+    )(*(pltpu.with_memory_space_constraint(x, pltpu.HBM) for x in operands))
     stored = pl.pallas_call(
         store_kernel,
         out_shape=[

time: 129 us -> 131 us (1.016); the launches traced: 128 us -> 129 us
  Pallas kernels: 120 us -> 128 us
  local copies, waits for them, and re-layouts: 7.9 us -> 0 us
    pallas_call x1, Pallas kernels: 117 us -> 125 us  [shards(): pl.pallas_call(functools.partial(step_kernel, n), out_shape=[out(count, w...]
    unnamed x18 -> x0, local copies, waits for them, and re-layouts: 7.9 us -> none
where the time goes in v4:
time: 131 us; the launch traced here: 129 us
  Pallas kernels  128 us (98%)
    pallas_call x1, Pallas kernels, shards(): pl.pallas_call(functools.partial(step_kernel, n), out_shape=[out(count, w...  125 us
    pallas_call x1, Pallas kernels, shards(): pl.pallas_call(store_kernel, out_shape=[out(count, width), out(count, cha...  3.07 us

profile of v4, /device:TPU:0, one launch (start us, length us, event | category | flops | bytes accessed | tf_op | source)
XLA Modules:
  0.0 128.9 jit_solution(16424445277524803394)
XLA Ops:
  0.6 125.2 %shard_map.188 = (bf16[256,512]{1,0:T(8,128)(2,1)S(1)}, bf16[3,256,256]{2,1,0:T(8,128)(2,1)S(1)}, f32[256,256]{1,0:T(8,128)S(1)}, f32[2048,256]{1,0:T(8,128)S(1)...) custom-call(bf16[256,2048]{1,0:T(8,128)(2,1)} %refs_0_.1, bf16[256,2048]{1,0:T(8,128)(2,1)} %refs_1_.1, ...), custom_call_target="tpu_custom_call" | custom-call | tf_op jit(solution)/shard_map/pallas_call | solution.py:825
  125.8 3.1 %shard_map.189 = (bf16[256,512]{1,0:T(8,128)(2,1)}, bf16[256,256]{1,0:T(8,128)(2,1)}, bf16[256,256]{1,0:T(8,128)(2,1)}, bf16[256,256]{1,0:T(8,128)(2,1)}, f32[25...) custom-call(bf16[256,512]{1,0:T(8,128)(2,1)S(1)} %get-tuple-element.22.stream, ...), custom_call_target="tpu_custom_call" | custom-call | tf_op jit(solution)/shard_map/pallas_call | solution.py:898

commit v5 on v4

--- a/solution.py
+++ b/solution.py
@@ -8,7 +8,7 @@
 from jax.sharding import PartitionSpec as P
 
 norm_eps = 1e-06
-VMEM = 42 * 1024 * 1024
+VMEM = 83 * 512 * 1024
 
 
 def rows_product(left, right):
@@ -56,9 +56,9 @@
     return (tp, cross, partner, lax.rem(partner + count // 2, count))
 
 
-def greet(cross, partner):
+def greet(peers):
     barrier = pltpu.get_barrier_semaphore()
-    for peer in (cross, partner):
+    for peer in peers:
         pl.semaphore_signal(barrier, inc=1, device_id={"tp": peer}, device_id_type=MESH)
     me, n = lax.axis_index("sp"), lax.axis_size("sp")
 
@@ -68,7 +68,7 @@
         return carry
 
     lax.fori_loop(1, n, greet_one, 0)
-    return lambda: pl.semaphore_wait(barrier, n + 1)
+    return lambda: pl.semaphore_wait(barrier, n - 1 + len(peers))
 
 
 def loop(low, high, body):
@@ -93,7 +93,6 @@
         down_sum,
         normed,
         inverse,
-        along,
         keys,
         weights,
         arrived,
@@ -111,6 +110,7 @@
         back,
         acc,
         token,
+        token_out,
         extended,
         filtered,
         extended_grad,
@@ -135,8 +135,9 @@
         out_send,
         out_recv,
         all_send,
-        all_cross,
-        all_near,
+        all_recv,
+        row_send,
+        row_recv,
         halo_send,
         halo_recv,
         mix_send,
@@ -173,19 +174,14 @@
     chunk = min(256, width)
     channels = filtered.shape[1]
     block = wide // n
-    shared_parts = wide // width
-    shared_parts = shared_parts if block % (16 * shared_parts) == 0 else 1
-    share = block // shared_parts
-    wait_all = greet(cross, partner)
+    wait_all = greet((cross, partner, diagonal))
     sources = (normed, cot)
-    edge = lax.rem(lax.div(me, max(1, n // 4)) + 1, 4) < 2
-    inner = jnp.logical_not(edge)
     loads = [
         pltpu.make_async_copy(source, target, load.at[i])
         for i, (source, target) in enumerate(zip(inputs, loaded))
     ]
-    for one in loads:
-        one.start()
+    for i in (3, 4, 1, 0, 2, 6, 7, 5, 8, 10, 11, 12, 9):
+        loads[i].start()
 
     def other(s):
         return mirrored(me, jnp.int32(s), n)
@@ -315,13 +311,29 @@
             mixed.at[source], mixed.at[target], mix_send, mix_recv.at[target], {"sp": other(k)}
         )
 
+    def send_own(a, k):
+        values = sources[a][:, columns(tp, width)]
+        sending[a, at(k), :] = chosen(a, 0, other(k), values)
+        slot_copy(a, k, k).start()
+
     with jax.named_scope("prep"):
+        loads[3].wait()
+        loads[4].wait()
+        table(0, choice, scales)
+        loads[1].wait()
+    with jax.named_scope("barrier"):
+        wait_all()
+    with jax.named_scope("send_own"):
+        loop(1, half, lambda k: send_own(1, k))
         loads[0].wait()
         loads[2].wait()
         loop(0, count // 32, normalize)
-        loads[3].wait()
-        loads[4].wait()
-        table(0, choice, scales)
+        loop(1, half, lambda k: send_own(0, k))
+        for one in route_copies():
+            one.start()
+        token_copy(0).start()
+        token_copy(1).start()
+    with jax.named_scope("conv"):
         loads[6].wait()
         loads[7].wait()
         product = in_gate[...].astype(jnp.float32) * conv_input[...].astype(jnp.float32)
@@ -334,28 +346,6 @@
         @pl.when(me == n - 1)
         def _():
             extended_grad[pl.ds(count, 8), :] = jnp.zeros((8, channels), jnp.float32)
-
-    with jax.named_scope("barrier"):
-        wait_all()
-        loads[1].wait()
-
-    def send_own(k):
-        for a in (0, 1):
-            values = sources[a][:, columns(tp, width)]
-            sending[a, at(k), :] = chosen(a, 0, other(k), values)
-            slot_copy(a, k, k).start()
-
-    with jax.named_scope("send_own"):
-        loop(1, group, send_own)
-
-        @pl.when(edge)
-        def _():
-            for one in route_copies():
-                one.start()
-            token_copy(0).start()
-            token_copy(1).start()
-
-        loop(group, half, send_own)
 
         @pl.when(me < n - 1)
         def _():
@@ -368,7 +358,7 @@
                 slots[a, pl.ds(0, depth), where] = chosen(a, 0, me, sources[a][:, where])
 
     def land(s, k):
-        for a in (0, 1):
+        for a in (1, 0):
             slot_copy(a, s, k).wait_recv()
             spread(a, s)
 
@@ -385,13 +375,6 @@
                     one.wait_recv()
                 table(1, arrived_choice, arrived_scales)
             token_copy(a).wait_recv()
-
-            @pl.when(inner)
-            def _():
-                if a == 0:
-                    for one in route_copies():
-                        one.start()
-                token_copy(a).start()
 
             def send_other(k):
                 sending[a, at(half + k), :] = chosen(a, 1, other(k), arrived[a])
@@ -525,45 +508,18 @@
         mixed[0] = (out_gate[...].astype(jnp.float32) * filtered[...]).astype(jnp.bfloat16)
 
     with jax.named_scope("land_first"):
-
-        @pl.when(inner)
-        def _():
-            take_tokens()
-            loop(1, group, land_other)
-            loop(group, half, land_own)
-
-        @pl.when(edge)
-        def _():
-            loop(group, half, land_own)
-
+        loop(group, half, land_own)
     for i in range(10, 13):
         loads[i].wait()
-    step(jnp.where(edge, 0, 2))
+    step(0)
     with jax.named_scope("land_second"):
-
-        @pl.when(inner)
-        def _():
-            pair_group(2)
-            loop(group, half, land_other)
-
-        @pl.when(edge)
-        def _():
-            take_tokens()
-            loop(1, half, land_other)
-
+        take_tokens()
+        loop(1, half, land_other)
     mix_early()
-    step(jnp.where(edge, 1, 0))
-    step(jnp.where(edge, 2, 1))
+    step(1)
+    step(2)
     with jax.named_scope("return_far"):
-
-        @pl.when(inner)
-        def _():
-            finish_group(2)
-
-        @pl.when(edge)
-        def _():
-            pair_group(2)
-
+        pair_group(2)
         mix_late()
     step(3)
     pieces_of = wide // chunk
@@ -571,11 +527,7 @@
         pair_group(0)
         pair_group(3)
         pair_group(1)
-
-        @pl.when(edge)
-        def _():
-            finish_group(2)
-
+        finish_group(2)
     with jax.named_scope("grads"):
         loop(0, pieces_of // 2, grads)
     with jax.named_scope("finish"):
@@ -596,74 +548,88 @@
 
     with jax.named_scope("combine"):
         loop(0, n, combine)
-    pieces = all_cross.shape[0]
-    tall = count // pieces
-
-    def shared(i, column, send, recv, peer):
-        part = token.at[pl.ds(i * tall, tall), columns(column, width)]
-        return remote(part, part, send, recv, {"tp": peer})
+    quarter = token.shape[0]
+
+    def quarter_rows(column):
+        return pl.ds(pl.multiple_of(column * quarter, quarter), quarter)
+
+    def exchange(j):
+        peer = (cross, diagonal, partner)[j]
+        return remote(
+            token_out.at[quarter_rows(peer)],
+            token.at[:, columns(tp, width)],
+            all_send.at[j],
+            all_recv.at[j],
+            {"tp": peer},
+        )
 
     with jax.named_scope("share"):
-        token[:, columns(tp, width)] = acc[...].astype(jnp.bfloat16)
-        for i in range(pieces):
-            shared(i, tp, all_send.at[0, i], all_cross.at[i], cross).start()
-            shared(i, tp, all_send.at[1, i], all_near.at[0, i], partner).start()
-        for i in range(pieces):
-            shared(i, cross, all_send.at[0, i], all_cross.at[i], cross).wait_recv()
-            shared(i, cross, all_send.at[2, i], all_near.at[1, i], partner).start()
-        for i in range(pieces):
-            for j in (0, 1):
-                shared(i, tp, all_send.at[j + 1, i], all_near.at[j, i], partner).wait()
-            shared(i, tp, all_send.at[0, i], all_cross.at[i], cross).wait_send()
-
-    def reduce_along(i):
-        rows = pl.ds(pl.multiple_of(i * 32, 32), 32)
-        unit = stream[rows, :].astype(jnp.float32) * inverse[rows, :]
-        unit_grad = token[rows, :].astype(jnp.float32) * gain[...]
-        along[rows, :] = jnp.mean(unit * unit_grad, axis=-1, keepdims=True)
-
-    def total_grad(c):
-        where = pl.ds(pl.multiple_of(c * chunk, chunk), chunk)
-        scale = inverse[...]
-        unit = stream[:, where].astype(jnp.float32) * scale
-        unit_grad = token[:, where].astype(jnp.float32) * gain[:, where]
-        value = cot[:, where].astype(jnp.float32) + scale * (unit_grad - unit * along[...])
+        token_out[...] = acc[...].astype(jnp.bfloat16)
+        for j in range(3):
+            exchange(j).start()
+        token[:, columns(tp, width)] = token_out[quarter_rows(tp), :]
+        for j in (2, 0, 1):
+            exchange(j).wait_recv()
+
+    def total_grad(i):
+        here = pl.ds(pl.multiple_of(i * 16, 16), 16)
+        rows = pl.ds(pl.multiple_of(tp * quarter + i * 16, 16), 16)
+        scale = inverse[rows, :]
+        unit = stream[rows, :].astype(jnp.float32) * scale
+        unit_grad = token[here, :].astype(jnp.float32) * gain[...]
+        along = jnp.mean(unit * unit_grad, axis=-1, keepdims=True)
+        value = cot[rows, :].astype(jnp.float32) + scale * (unit_grad - unit * along)
         value = value.astype(jnp.bfloat16)
-        stream_grad[:, where] = value
-        turned[where, :] = jnp.transpose(value.astype(jnp.float32)).astype(jnp.bfloat16)
+        stream_grad[rows, :] = value
+        for owner in range(n):
+            turned[owner, here, :] = value[:, owner * block : (owner + 1) * block]
 
     with jax.named_scope("stream_grad"):
-        loop(0, count // 32, reduce_along)
-        loop(0, wide // chunk, total_grad)
-
-    def turned_rows(owner, part):
-        return pl.ds(pl.multiple_of(owner * block + part * share, share), share)
-
-    def part_rows(part):
-        return pl.ds(pl.multiple_of(part * share, share), share)
-
-    mine_part = tp if shared_parts > 1 else 0
-    cross_part = cross if shared_parts > 1 else 0
+        loop(0, quarter // 16, total_grad)
 
     def turn_copy(s):
         return remote(
-            turned.at[turned_rows(other(s), mine_part)],
-            turned_all.at[s, part_rows(mine_part)],
+            turned.at[other(s)],
+            turned_all.at[s, quarter_rows(tp)],
             turn_send.at[0],
             turn_recv.at[s],
             {"sp": other(s)},
         )
 
-    def turn_part(s, part, send, recv, peer):
-        rows = turned_all.at[s, part_rows(part)]
+    def turn_part(s, column, send, recv, peer):
+        rows = turned_all.at[s, quarter_rows(column)]
         return remote(rows, rows, send, recv, {"tp": peer})
 
-    def turn_start(k):
-        turn_copy(n - k).start()
-
+    def gather(column, j, recv, peer):
+        rows = stream_grad.at[quarter_rows(column)]
+        return remote(rows, rows, row_send.at[j], row_recv.at[recv], {"tp": peer})
+
+    def turn_spread(s):
+        turn_part(s, tp, turn_send.at[1], turn_cross.at[s], cross).start()
+        turn_part(s, tp, turn_send.at[2], turn_near.at[s], partner).start()
+
+    def turn_land(s):
+        turn_copy(s).wait_recv()
+        turn_spread(s)
+
+    def turn_forward(s):
+        turn_part(s, cross, turn_send.at[1], turn_cross.at[s], cross).wait_recv()
+        turn_part(s, cross, turn_send.at[3], turn_near.at[s], partner).start()
+
+    with jax.named_scope("turn_start"):
+        loop(1, n, lambda k: turn_copy(n - k).start())
+        gather(tp, 0, 0, cross).start()
+        gather(tp, 1, 1, partner).start()
+        turned_all[0, quarter_rows(tp), :] = turned[me]
+        turn_spread(0)
+    with jax.named_scope("gather"):
+        gather(cross, 0, 0, cross).wait_recv()
+        gather(cross, 2, 2, partner).start()
+    with jax.named_scope("turn_land"):
+        loop(1, n, turn_land)
     with jax.named_scope("mixed_grad"):
-        loop(1, n, turn_start)
-        stream_out[...] = stream_grad[:, columns(tp, width)]
+        gather(tp, 1, 1, partner).wait_recv()
+        gather(tp, 2, 2, partner).wait_recv()
         loads[9].wait()
         mixed_grad = jnp.dot(stream_grad[...], w_out[...], preferred_element_type=jnp.float32)
         small_out[0] = (mixed_grad * filtered[...]).astype(jnp.bfloat16)
@@ -673,22 +639,9 @@
         def _():
             halo_earlier().start()
 
-    def turn_land(s):
-        turn_copy(s).wait_recv()
-        if shared_parts > 1:
-            turn_part(s, tp, turn_send.at[1], turn_cross.at[s], cross).start()
-            turn_part(s, tp, turn_send.at[2], turn_near.at[s], partner).start()
-
-    def turn_forward(s):
-        turn_part(s, cross, turn_send.at[1], turn_cross.at[s], cross).wait_recv()
-        turn_part(s, cross, turn_send.at[3], turn_near.at[s], partner).start()
-
-    with jax.named_scope("turn_land"):
-        loop(1, n, turn_land)
+        stream_out[...] = stream_grad[:, columns(tp, width)]
     with jax.named_scope("turn_forward"):
-        if shared_parts > 1:
-            loop(1, n, turn_forward)
-
+        loop(0, n, turn_forward)
     with jax.named_scope("conv_grad"):
         @pl.when(me < n - 1)
         def _():
@@ -702,20 +655,13 @@
         small_out[1] = (product_grad * conv_input[...].astype(jnp.float32)).astype(jnp.bfloat16)
         small_out[2] = (product_grad * in_gate[...].astype(jnp.float32)).astype(jnp.bfloat16)
 
-    w_out_sum[...] = jnp.dot(
-        turned[pl.ds(pl.multiple_of(me * block, block), block), :],
-        mixed[0],
-        preferred_element_type=jnp.float32,
-    )
+    w_out_sum[...] = jnp.zeros_like(w_out_sum)
 
     def out_step(s):
-        if shared_parts > 1:
-            pair_rows = turned_all.at[s, pl.ds(0, 2 * share)]
-            remote(
-                pair_rows, pair_rows, turn_send.at[2], turn_near.at[s], {"tp": partner}
-            ).wait_recv()
-
-        @pl.when(s < half)
+        both = turned_all.at[s, pl.ds(0, 2 * quarter)]
+        remote(both, both, turn_send.at[2], turn_near.at[s], {"tp": partner}).wait_recv()
+
+        @pl.when((s > 0) & (s < half))
         def _():
             mix_copy(0, s, s).wait_recv()
 
@@ -723,10 +669,10 @@
         def _():
             mix_copy(half, s, s - half).wait_recv()
 
-        w_out_sum[...] += jnp.dot(turned_all[s], mixed[s], preferred_element_type=jnp.float32)
+        w_out_sum[...] += rows_product(turned_all[s], mixed[s])
 
     with jax.named_scope("w_out_grad"):
-        loop(1, n, out_step)
+        loop(0, n, out_step)
 
     with jax.named_scope("drain"):
         for one in route_copies():
@@ -744,9 +690,14 @@
         remote(rest, rest, out_send, out_recv.at[0], {"tp": partner}).wait_send()
         sent = mixed.at[pl.ds(0, n - 1)]
         remote(sent, sent, mix_send, mix_recv.at[0], {"tp": partner}).wait_send()
-        sent = turned_all.at[pl.ds(0, n - 1), pl.ds(0, share)]
-        for kind in range(4 if shared_parts > 1 else 1):
+        sent = turned_all.at[pl.ds(0, n - 1), pl.ds(0, quarter)]
+        remote(sent, sent, turn_send.at[0], turn_recv.at[0], {"tp": partner}).wait_send()
+        sent = turned_all.at[:, pl.ds(0, quarter)]
+        for kind in range(1, 4):
             remote(sent, sent, turn_send.at[kind], turn_recv.at[0], {"tp": partner}).wait_send()
+        for j in range(3):
+            exchange(j).wait_send()
+            gather(tp, j, j, partner).wait_send()
 
         @pl.when(me < n - 1)
         def _():
@@ -793,7 +744,7 @@
     depth = 4 * count // n
     rows = n * depth
     block = wide // n
-    pieces = 2
+    quarter = count // lax.axis_size("tp")
     kind = stream_in.dtype
 
     def out(*shape, dtype=kind):
@@ -838,7 +789,6 @@
         + [
             held(count, wide),
             full(count, 1),
-            full(count, 1),
             full(2, n, count),
             full(2, n, count),
             held(2, count, width),
@@ -855,14 +805,15 @@
             held(rows, width),
             held(rows, width),
             full(count, width),
-            held(count, wide),
+            held(quarter, wide),
+            held(count, width),
             full(count + 8, channels),
             full(count, channels),
             full(count + 8, channels),
             held(n, count, channels),
             held(count, wide),
-            held(wide, count),
-            held(n, block, count),
+            held(n, quarter, block),
+            held(n, count, block),
             dma((13,)),
             dma((4,)),
             dma((4,)),
@@ -879,9 +830,10 @@
             dma((n,)),
             dma,
             dma((n,)),
-            dma((3, pieces)),
-            dma((pieces,)),
-            dma((2, pieces)),
+            dma((3,)),
+            dma((3,)),
+            dma((3,)),
+            dma((3,)),
             dma((2,)),
             dma((2,)),
             dma,
@@ -892,7 +844,7 @@
             dma((n,)),
         ],
         compiler_params=pltpu.CompilerParams(
-            collective_id=1, has_side_effects=True, vmem_limit_bytes=VMEM + 2 * n * count * channels
+            collective_id=1, has_side_effects=True, vmem_limit_bytes=VMEM + 3 * n * count * channels
         ),
     )(*(pltpu.with_memory_space_constraint(x, pltpu.HBM) for x in operands))
     stored = pl.pallas_call(

time: 131 us -> 121 us (0.924); the launches traced: 129 us -> 121 us
  Pallas kernels: 128 us -> 120 us
    pallas_call x1, Pallas kernels: 125 us -> 117 us  [shards(): pl.pallas_call(functools.partial(step_kernel, n), out_shape=[out(count, w...]
where the time goes in v5:
time: 121 us
  Pallas kernels  120 us (99%)
    pallas_call x1, Pallas kernels, shards(): pl.pallas_call(functools.partial(step_kernel, n), out_shape=[out(count, w...  117 us
    pallas_call x1, Pallas kernels, shards(): pl.pallas_call(store_kernel, out_shape=[out(count, width), out(count, cha...  3.07 us

profile of v5, /device:TPU:0, one launch (start us, length us, event | category | flops | bytes accessed | tf_op | source)
XLA Modules:
  0.0 121.1 jit_solution(17056897210699561990)
XLA Ops:
  0.6 117.4 %shard_map.188 = (bf16[256,512]{1,0:T(8,128)(2,1)S(1)}, bf16[3,256,256]{2,1,0:T(8,128)(2,1)S(1)}, f32[256,256]{1,0:T(8,128)S(1)}, f32[2048,256]{1,0:T(8,128)S(1)...) custom-call(bf16[256,2048]{1,0:T(8,128)(2,1)} %refs_0_.1, bf16[256,2048]{1,0:T(8,128)(2,1)} %refs_1_.1, ...), custom_call_target="tpu_custom_call" | custom-call | tf_op jit(solution)/shard_map/pallas_call | solution.py:776
  118.0 3.1 %shard_map.189 = (bf16[256,512]{1,0:T(8,128)(2,1)}, bf16[256,256]{1,0:T(8,128)(2,1)}, bf16[256,256]{1,0:T(8,128)(2,1)}, bf16[256,256]{1,0:T(8,128)(2,1)}, f32[25...) custom-call(bf16[256,512]{1,0:T(8,128)(2,1)S(1)} %get-tuple-element.22.stream, ...), custom_call_target="tpu_custom_call" | custom-call | tf_op jit(solution)/shard_map/pallas_call | solution.py:850

commit v6 on v5

--- a/solution.py
+++ b/solution.py
@@ -324,53 +324,45 @@
     with jax.named_scope("barrier"):
         wait_all()
     with jax.named_scope("send_own"):
+        for one in route_copies():
+            one.start()
         loop(1, half, lambda k: send_own(1, k))
+        token_copy(1).start()
+        with jax.named_scope("conv"):
+            loads[6].wait()
+            loads[7].wait()
+            product = in_gate[...].astype(jnp.float32) * conv_input[...].astype(jnp.float32)
+            extended[pl.ds(8, count), :] = product
+
+            @pl.when(me == 0)
+            def _():
+                extended[pl.ds(0, 8), :] = jnp.zeros((8, channels), jnp.float32)
+
+            @pl.when(me == n - 1)
+            def _():
+                extended_grad[pl.ds(count, 8), :] = jnp.zeros((8, channels), jnp.float32)
+
+            @pl.when(me < n - 1)
+            def _():
+                halo_later().start()
         loads[0].wait()
         loads[2].wait()
         loop(0, count // 32, normalize)
         loop(1, half, lambda k: send_own(0, k))
-        for one in route_copies():
-            one.start()
         token_copy(0).start()
-        token_copy(1).start()
-    with jax.named_scope("conv"):
-        loads[6].wait()
-        loads[7].wait()
-        product = in_gate[...].astype(jnp.float32) * conv_input[...].astype(jnp.float32)
-        extended[pl.ds(8, count), :] = product
-
-        @pl.when(me == 0)
-        def _():
-            extended[pl.ds(0, 8), :] = jnp.zeros((8, channels), jnp.float32)
-
-        @pl.when(me == n - 1)
-        def _():
-            extended_grad[pl.ds(count, 8), :] = jnp.zeros((8, channels), jnp.float32)
-
-        @pl.when(me < n - 1)
-        def _():
-            halo_later().start()
-
     with jax.named_scope("own_block"):
         for a in (0, 1):
             for piece in range(wide // width):
                 where = pl.ds(piece * width, width)
                 slots[a, pl.ds(0, depth), where] = chosen(a, 0, me, sources[a][:, where])
 
-    def land(s, k):
+    def land(a, s, k):
+        slot_copy(a, s, k).wait_recv()
+        spread(a, s)
+
+    def take_tokens():
         for a in (1, 0):
-            slot_copy(a, s, k).wait_recv()
-            spread(a, s)
-
-    def land_own(k):
-        land(k, k)
-
-    def land_other(k):
-        land(half + k, k)
-
-    def take_tokens():
-        for a in (0, 1):
-            if a == 0:
+            if a == 1:
                 for one in route_copies():
                     one.wait_recv()
                 table(1, arrived_choice, arrived_scales)
@@ -491,8 +483,22 @@
 
         loop(0, group, one)
 
-    with jax.named_scope("land_near"):
-        loop(1, group, land_own)
+    with jax.named_scope("land_first"):
+        for a in (1, 0):
+            loop(1, half, lambda k: land(a, k, k))
+    for i in range(10, 13):
+        loads[i].wait()
+    with jax.named_scope("tokens"):
+        take_tokens()
+    with jax.named_scope("land_second"):
+        for a in (1,):
+            loop(1, half, lambda k: land(a, half + k, k))
+    step(0)
+    with jax.named_scope("land_second"):
+        for a in (0,):
+            loop(1, half, lambda k: land(a, half + k, k))
+    with jax.named_scope("pair0"):
+        pair_group(0)
     with jax.named_scope("filter"):
         @pl.when(me > 0)
         def _():
@@ -507,35 +513,34 @@
         )
         mixed[0] = (out_gate[...].astype(jnp.float32) * filtered[...]).astype(jnp.bfloat16)
 
-    with jax.named_scope("land_first"):
-        loop(group, half, land_own)
-    for i in range(10, 13):
-        loads[i].wait()
-    step(0)
-    with jax.named_scope("land_second"):
-        take_tokens()
-        loop(1, half, land_other)
     mix_early()
+    pieces_of = wide // chunk
     step(1)
     step(2)
-    with jax.named_scope("return_far"):
+    with jax.named_scope("pair2"):
         pair_group(2)
-        mix_late()
+    mix_late()
     step(3)
-    pieces_of = wide // chunk
-    with jax.named_scope("pairs"):
-        pair_group(0)
+    with jax.named_scope("pair3"):
         pair_group(3)
+    with jax.named_scope("pair1"):
         pair_group(1)
+    with jax.named_scope("fin0"):
+        finish_group(0)
+    with jax.named_scope("fin2"):
         finish_group(2)
     with jax.named_scope("grads"):
-        loop(0, pieces_of // 2, grads)
-    with jax.named_scope("finish"):
-        finish_group(0)
+        loop(0, pieces_of // 4, grads)
+    with jax.named_scope("grads"):
+        loop(pieces_of // 4, pieces_of // 2, grads)
+    with jax.named_scope("fin3"):
         finish_group(3)
+    with jax.named_scope("fin1"):
         finish_group(1)
     with jax.named_scope("grads"):
-        loop(pieces_of // 2, pieces_of, grads)
+        loop(pieces_of // 2, 3 * pieces_of // 4, grads)
+    with jax.named_scope("grads"):
+        loop(3 * pieces_of // 4, pieces_of, grads)
     acc[...] = jnp.zeros_like(acc)
 
     def combine(s):

time: 121 us -> 114 us (0.942)
  Pallas kernels: 120 us -> 113 us
    pallas_call x1, Pallas kernels: 117 us -> 110 us  [shards(): pl.pallas_call(functools.partial(step_kernel, n), out_shape=[out(count, w...]
where the time goes in v6:
time: 114 us
  Pallas kernels  113 us (99%)
    pallas_call x1, Pallas kernels, shards(): pl.pallas_call(functools.partial(step_kernel, n), out_shape=[out(count, w...  110 us
    pallas_call x1, Pallas kernels, shards(): pl.pallas_call(store_kernel, out_shape=[out(count, width), out(count, cha...  3.07 us

profile of v6, /device:TPU:0, one launch (start us, length us, event | category | flops | bytes accessed | tf_op | source)
XLA Modules:
  0.0 113.9 jit_solution(2989274430673266473)
XLA Ops:
  0.6 110.2 %shard_map.188 = (bf16[256,512]{1,0:T(8,128)(2,1)S(1)}, bf16[3,256,256]{2,1,0:T(8,128)(2,1)S(1)}, f32[256,256]{1,0:T(8,128)S(1)}, f32[2048,256]{1,0:T(8,128)S(1)...) custom-call(bf16[256,2048]{1,0:T(8,128)(2,1)} %refs_0_.1, bf16[256,2048]{1,0:T(8,128)(2,1)} %refs_1_.1, ...), custom_call_target="tpu_custom_call" | custom-call | tf_op jit(solution)/shard_map/pallas_call | solution.py:781
  110.8 3.1 %shard_map.189 = (bf16[256,512]{1,0:T(8,128)(2,1)}, bf16[256,256]{1,0:T(8,128)(2,1)}, bf16[256,256]{1,0:T(8,128)(2,1)}, bf16[256,256]{1,0:T(8,128)(2,1)}, f32[25...) custom-call(bf16[256,512]{1,0:T(8,128)(2,1)S(1)} %get-tuple-element.22.stream, ...), custom_call_target="tpu_custom_call" | custom-call | tf_op jit(solution)/shard_map/pallas_call | solution.py:855

commit v7 on v6

--- a/solution.py
+++ b/solution.py
@@ -316,6 +316,28 @@
         sending[a, at(k), :] = chosen(a, 0, other(k), values)
         slot_copy(a, k, k).start()
 
+    def next_copy(a):
+        return remote(
+            sending.at[a, at(0)],
+            slots.at[a, at(1), columns(cross, width)],
+            slot_send.at[a],
+            slot_recv.at[a, 1],
+            {"sp": other(1)},
+        )
+
+    def send_next(a):
+        send_own(a, 1)
+        values = sources[a][:, columns(cross, width)]
+        sending[a, at(0), :] = chosen(a, 0, other(1), values)
+        next_copy(a).start()
+
+    def land_next(a):
+        both = slots.at[a, at(1), pl.ds(0, 2 * width)]
+        remote(both, both, slot_send.at[a], slot_recv.at[a, 1], {"sp": other(1)}).wait_recv()
+        for column, sem in ((tp, near_send), (cross, fwd_send)):
+            part = slots.at[a, at(1), columns(column, width)]
+            remote(part, part, sem.at[a], near_recv.at[a, 1], {"tp": partner}).start()
+
     with jax.named_scope("prep"):
         loads[3].wait()
         loads[4].wait()
@@ -326,7 +348,8 @@
     with jax.named_scope("send_own"):
         for one in route_copies():
             one.start()
-        loop(1, half, lambda k: send_own(1, k))
+        loop(2, half, lambda k: send_own(1, k))
+        send_next(1)
         token_copy(1).start()
         with jax.named_scope("conv"):
             loads[6].wait()
@@ -348,7 +371,8 @@
         loads[0].wait()
         loads[2].wait()
         loop(0, count // 32, normalize)
-        loop(1, half, lambda k: send_own(0, k))
+        loop(2, half, lambda k: send_own(0, k))
+        send_next(0)
         token_copy(0).start()
     with jax.named_scope("own_block"):
         for a in (0, 1):
@@ -441,7 +465,7 @@
         def forward_one(i):
             s = g * group + i
 
-            @pl.when(s > 0)
+            @pl.when(s > 1)
             def _():
                 forward_both(s)
 
@@ -485,7 +509,8 @@
 
     with jax.named_scope("land_first"):
         for a in (1, 0):
-            loop(1, half, lambda k: land(a, k, k))
+            loop(2, half, lambda k: land(a, k, k))
+            land_next(a)
     for i in range(10, 13):
         loads[i].wait()
     with jax.named_scope("tokens"):
@@ -521,10 +546,10 @@
         pair_group(2)
     mix_late()
     step(3)
+    with jax.named_scope("pair1"):
+        pair_group(1)
     with jax.named_scope("pair3"):
         pair_group(3)
-    with jax.named_scope("pair1"):
-        pair_group(1)
     with jax.named_scope("fin0"):
         finish_group(0)
     with jax.named_scope("fin2"):
@@ -533,10 +558,10 @@
         loop(0, pieces_of // 4, grads)
     with jax.named_scope("grads"):
         loop(pieces_of // 4, pieces_of // 2, grads)
+    with jax.named_scope("fin1"):
+        finish_group(1)
     with jax.named_scope("fin3"):
         finish_group(3)
-    with jax.named_scope("fin1"):
-        finish_group(1)
     with jax.named_scope("grads"):
         loop(pieces_of // 2, 3 * pieces_of // 4, grads)
     with jax.named_scope("grads"):
@@ -684,11 +709,13 @@
             one.wait_send()
         for a in (0, 1):
             token_copy(a).wait_send()
-            sent = sending.at[a, pl.ds(0, (n - 2) * depth)]
+            sent = sending.at[a, pl.ds(0, (n - 1) * depth)]
             remote(sent, sent, slot_send.at[a], slot_recv.at[a, 0], {"tp": partner}).wait_send()
             most = slots.at[a, pl.ds(0, (n - 1) * depth), pl.ds(0, width)]
-            for sem in (cross_send, near_send, fwd_send):
+            for sem in (near_send, fwd_send):
                 remote(most, most, sem.at[a], near_recv.at[a, 0], {"tp": partner}).wait_send()
+            most = slots.at[a, pl.ds(0, (n - 2) * depth), pl.ds(0, width)]
+            remote(most, most, cross_send.at[a], near_recv.at[a, 0], {"tp": cross}).wait_send()
             remote(far_out, far_in, hand_send.at[a], hand_recv.at[a, 0], {"tp": partner}).wait_send()
         remote(far_out, far_in, far_send, far_recv.at[0], {"tp": cross}).wait_send()
         rest = total.at[pl.ds(0, (n - 1) * depth)]

time: 114 us -> 112 us (0.982)
  Pallas kernels: 113 us -> 111 us
    pallas_call x1, Pallas kernels: 110 us -> 108 us  [shards(): pl.pallas_call(functools.partial(step_kernel, n), out_shape=[out(count, w...]
where the time goes in v7:
time: 112 us
  Pallas kernels  111 us (99%)
    pallas_call x1, Pallas kernels, shards(): pl.pallas_call(functools.partial(step_kernel, n), out_shape=[out(count, w...  108 us
    pallas_call x1, Pallas kernels, shards(): pl.pallas_call(store_kernel, out_shape=[out(count, width), out(count, cha...  3.07 us

profile of v7, /device:TPU:0, one launch (start us, length us, event | category | flops | bytes accessed | tf_op | source)
XLA Modules:
  0.0 111.8 jit_solution(2176688077884896536)
XLA Ops:
  0.6 108.0 %shard_map.188 = (bf16[256,512]{1,0:T(8,128)(2,1)S(1)}, bf16[3,256,256]{2,1,0:T(8,128)(2,1)S(1)}, f32[256,256]{1,0:T(8,128)S(1)}, f32[2048,256]{1,0:T(8,128)S(1)...) custom-call(bf16[256,2048]{1,0:T(8,128)(2,1)} %refs_0_.1, bf16[256,2048]{1,0:T(8,128)(2,1)} %refs_1_.1, ...), custom_call_target="tpu_custom_call" | custom-call | tf_op jit(solution)/shard_map/pallas_call | solution.py:808
  108.7 3.1 %shard_map.189 = (bf16[256,512]{1,0:T(8,128)(2,1)}, bf16[256,256]{1,0:T(8,128)(2,1)}, bf16[256,256]{1,0:T(8,128)(2,1)}, bf16[256,256]{1,0:T(8,128)(2,1)}, f32[25...) custom-call(bf16[256,512]{1,0:T(8,128)(2,1)S(1)} %get-tuple-element.22.stream, ...), custom_call_target="tpu_custom_call" | custom-call | tf_op jit(solution)/shard_map/pallas_call | solution.py:882

commit v8 on v7

--- a/solution.py
+++ b/solution.py
@@ -648,15 +648,15 @@
 
     with jax.named_scope("turn_start"):
         loop(1, n, lambda k: turn_copy(n - k).start())
-        gather(tp, 0, 0, cross).start()
         gather(tp, 1, 1, partner).start()
         turned_all[0, quarter_rows(tp), :] = turned[me]
         turn_spread(0)
+        gather(tp, 0, 0, cross).start()
+    with jax.named_scope("turn_land"):
+        loop(1, n, turn_land)
     with jax.named_scope("gather"):
         gather(cross, 0, 0, cross).wait_recv()
         gather(cross, 2, 2, partner).start()
-    with jax.named_scope("turn_land"):
-        loop(1, n, turn_land)
     with jax.named_scope("mixed_grad"):
         gather(tp, 1, 1, partner).wait_recv()
         gather(tp, 2, 2, partner).wait_recv()

time: 112 us -> 111 us (level)
  no operation moved by 1% of the time
where the time goes in v8:
time: 111 us
  Pallas kernels  110 us (99%)
    pallas_call x1, Pallas kernels, shards(): pl.pallas_call(functools.partial(step_kernel, n), out_shape=[out(count, w...  107 us
    pallas_call x1, Pallas kernels, shards(): pl.pallas_call(store_kernel, out_shape=[out(count, width), out(count, cha...  3.07 us

profile of v8, /device:TPU:0, one launch (start us, length us, event | category | flops | bytes accessed | tf_op | source)
XLA Modules:
  0.0 111.1 jit_solution(9657132368225052701)
XLA Ops:
  0.6 107.4 %shard_map.188 = (bf16[256,512]{1,0:T(8,128)(2,1)S(1)}, bf16[3,256,256]{2,1,0:T(8,128)(2,1)S(1)}, f32[256,256]{1,0:T(8,128)S(1)}, f32[2048,256]{1,0:T(8,128)S(1)...) custom-call(bf16[256,2048]{1,0:T(8,128)(2,1)} %refs_0_.1, bf16[256,2048]{1,0:T(8,128)(2,1)} %refs_1_.1, ...), custom_call_target="tpu_custom_call" | custom-call | tf_op jit(solution)/shard_map/pallas_call | solution.py:808
  108.0 3.1 %shard_map.189 = (bf16[256,512]{1,0:T(8,128)(2,1)}, bf16[256,256]{1,0:T(8,128)(2,1)}, bf16[256,256]{1,0:T(8,128)(2,1)}, bf16[256,256]{1,0:T(8,128)(2,1)}, f32[25...) custom-call(bf16[256,512]{1,0:T(8,128)(2,1)S(1)} %get-tuple-element.22.stream, ...), custom_call_target="tpu_custom_call" | custom-call | tf_op jit(solution)/shard_map/pallas_call | solution.py:882
